TPU v7x, 128 devices: a whole 4x4x4 slice. The times are simulated.
128 devices in a mesh: sp: 32 (over z, y, core), tp: 4 (over x).
Axes of the slice: x: 4, y: 4, z: 4, core: 2. Of those that a mesh axis runs over, the one named last changes fastest.
Arguments:
- query_nope: bfloat16 [6144, 4096], P('sp', 'tp'), may hold values from -6 to 6
- query_rope: bfloat16 [6144, 2048], P('sp', 'tp'), may hold values from -24 to 24
- latent: bfloat16 [6144, 512], P('sp'), may hold values from -6 to 6
- key_rope: bfloat16 [6144, 32], P('sp'), may hold values from -24 to 24
- latent_gain: float32 [512], replicated, may hold values from 0.1 to 1.9
- key_up: bfloat16 [512, 4096], P(None, 'tp'), may hold values from -0.25 to 0.25
- value_up: bfloat16 [512, 4096], P(None, 'tp'), may hold values from -0.25 to 0.25
- out_proj: bfloat16 [4096, 4096], P('tp'), may hold values from -0.09375 to 0.09375
- resid: bfloat16 [6144, 4096], P(('sp', 'tp')), may hold values from -6 to 6
- attn_gain: float32 [4096], replicated, may hold values from 0.1 to 1.9
- pre_gain: float32 [4096], replicated, may hold values from 0.1 to 1.9
- routes: int32 [6144, 2], P(('sp', 'tp')), may hold values from 0 to 31, all different within a row; in each aligned block of 48 rows (0 to 47, 48 to 95, ...) at most 6 rows name the same one
- route_weights: float32 [6144, 2], P(('sp', 'tp')), may hold values from 0.2 to 2
- expert_gate: bfloat16 [32, 4096, 1024], P('sp', None, 'tp'), may hold values from -0.09375 to 0.09375
- expert_up: bfloat16 [32, 4096, 1024], P('sp', None, 'tp'), may hold values from -0.09375 to 0.09375
- expert_down: bfloat16 [32, 1024, 4096], P('sp', 'tp'), may hold values from -0.1875 to 0.1875
- shared_gate: bfloat16 [4096, 1024], P(None, 'tp'), may hold values from -0.09375 to 0.09375
- shared_up: bfloat16 [4096, 1024], P(None, 'tp'), may hold values from -0.09375 to 0.09375
- shared_down: bfloat16 [1024, 4096], P('tp'), may hold values from -0.1875 to 0.1875
- moe_gain: float32 [4096], replicated, may hold values from 0.1 to 1.9
Outputs:
- output: bfloat16 [6144, 4096], P(('sp', 'tp'))
Inputs may be any that keep to these rules, and one draw needn't show every extreme that they name: `routes`: A row names 2 different experts. In each aligned block of 48 rows no expert is named by more than 6 rows, and in some block an expert is named by exactly 6 rows.
All inputs are finite; a program needn't handle non-finite values.
Results may differ from a plain program's by a relative error of at most 0.018.
Values may be sent and summed in bfloat16 or wider, within the bound.
A program may use at most 128 MiB of HBM per device.

v0:
```python
import math

import jax
import jax.numpy as jnp
from jax import lax
from jax.sharding import PartitionSpec as P

MODEL_DIM = 4096
NOPE_DIM = 64
ROPE_DIM = 32
VALUE_DIM = 64
TOP_K = 2


epsilon = 1e-06
theta_base = 10000.0


def cut_along(array, dim, count):
    before, after = (array.shape[:dim], array.shape[dim + 1 :])
    return jnp.moveaxis(array.reshape(*before, count, -1, *after), dim, 0)


def sum_at_owner(array, axis, dim):
    count = lax.axis_size(axis)
    blocks = lax.all_to_all(cut_along(array, dim, count), axis, 0, 0, tiled=True)
    return jnp.sum(blocks.astype(jnp.float32), axis=0)


def rms_scale(values, gain_vector):
    return (
        values
        * lax.rsqrt(jnp.mean(values * values, axis=-1, keepdims=True) + epsilon)
        * gain_vector
    )


def rotate(values, positions):
    half_dim = values.shape[-1] // 2
    inverse = theta_base ** (-jnp.arange(half_dim, dtype=jnp.float32) / half_dim)
    angles = positions.astype(jnp.float32)[..., None] * inverse
    cosine = jnp.cos(angles)
    sine_part = jnp.sin(angles)
    first_half = values[..., :half_dim]
    second_half = values[..., half_dim:]
    return jnp.concatenate(
        [
            first_half * cosine - second_half * sine_part,
            second_half * cosine + first_half * sine_part,
        ],
        axis=-1,
    )


def expert_block(expert_in, gate_part, up_part, down_part):
    hidden = (
        jax.nn.silu(jnp.dot(expert_in, gate_part, preferred_element_type=jnp.float32))
        * jnp.dot(expert_in, up_part, preferred_element_type=jnp.float32)
    ).astype(jnp.bfloat16)
    return jnp.dot(hidden, down_part, preferred_element_type=jnp.float32).astype(jnp.bfloat16)


def dispatch_table(normed_rows, route_rows, experts, capacity):
    row_count = normed_rows.shape[0]
    flat_routes = route_rows.reshape(-1)
    onehot = (flat_routes[:, None] == jnp.arange(experts, dtype=jnp.int32)[None, :]).astype(
        jnp.int32
    )
    earlier = jnp.cumsum(onehot, axis=0) - onehot
    target = flat_routes * capacity + jnp.sum(earlier * onehot, axis=1)
    matches = (
        target.reshape(row_count, -1)[None, :, :]
        == jnp.arange(experts * capacity, dtype=jnp.int32)[:, None, None]
    )
    spread = jnp.any(matches, axis=2).astype(jnp.bfloat16)
    slot_table = jnp.dot(spread, normed_rows, preferred_element_type=jnp.float32).astype(
        jnp.bfloat16
    )
    return (slot_table.reshape(experts, capacity, normed_rows.shape[1]), target)


def on_device(
    query_nope,
    query_rope,
    latent,
    key_rope,
    latent_gain,
    key_up,
    value_up,
    out_proj,
    resid,
    attn_gain,
    pre_gain,
    routes,
    route_weights,
    expert_gate,
    expert_up,
    expert_down,
    shared_gate,
    shared_up,
    shared_down,
    moe_gain,
):
    local_rows = query_nope.shape[0]
    heads_here = query_nope.shape[1] // NOPE_DIM
    query_pos = lax.axis_index("sp") * local_rows + jnp.arange(local_rows, dtype=jnp.int32)
    last_query = lax.axis_index("sp") * local_rows + local_rows - 1
    query_rot = rotate(
        query_rope.astype(jnp.float32).reshape(local_rows, heads_here, ROPE_DIM), query_pos[:, None]
    ).astype(jnp.bfloat16)
    key_rot = rotate(key_rope.astype(jnp.float32), query_pos).astype(jnp.bfloat16)
    latent_normed = rms_scale(latent.astype(jnp.float32), latent_gain).astype(jnp.bfloat16)
    query_heads = query_nope.reshape(local_rows, heads_here, NOPE_DIM)
    score_scale = (NOPE_DIM + ROPE_DIM) ** (-0.5)

    def attend(state_now, latent_rows, rotary_rows, key_start):
        piece_rows = latent_rows.shape[0]
        keys_here = jnp.dot(latent_rows, key_up, preferred_element_type=jnp.float32).astype(
            jnp.bfloat16
        )
        keys_here = keys_here.reshape(piece_rows, heads_here, NOPE_DIM)
        values_here = jnp.dot(latent_rows, value_up, preferred_element_type=jnp.float32).astype(
            jnp.bfloat16
        )
        values_here = values_here.reshape(piece_rows, heads_here, VALUE_DIM)
        scores = (
            jnp.einsum("qhd,khd->hqk", query_heads, keys_here, preferred_element_type=jnp.float32)
            + jnp.einsum("qhr,kr->hqk", query_rot, rotary_rows, preferred_element_type=jnp.float32)
        ) * score_scale
        allowed = (key_start + jnp.arange(piece_rows, dtype=jnp.int32))[None, :] <= query_pos[
            :, None
        ]
        scores = jnp.where(allowed[None], scores, -1e30)
        running, total_sum, summed = state_now
        newest = jnp.maximum(running, jnp.max(scores, axis=-1))
        factor = jnp.exp(running - newest)
        exponent = jnp.exp(scores - newest[..., None])
        total_sum = total_sum * factor + jnp.sum(exponent, axis=-1)
        summed = summed * factor[..., None] + jnp.einsum(
            "hqk,khd->hqd",
            exponent.astype(jnp.bfloat16),
            values_here,
            preferred_element_type=jnp.float32,
        )
        return (newest, total_sum, summed)

    initial = (
        jnp.full((heads_here, local_rows), -1e30, jnp.float32),
        jnp.zeros((heads_here, local_rows), jnp.float32),
        jnp.zeros((heads_here, local_rows, VALUE_DIM), jnp.float32),
    )
    latent_piece = lax.all_gather(latent_normed, "sp", axis=0, tiled=True)
    rotary_piece = lax.all_gather(key_rot, "sp", axis=0, tiled=True)
    piece_rows = latent_piece.shape[0]
    step_rows = math.gcd(piece_rows, 512)

    def one_step(step_index, inner_state):
        offset = step_index * step_rows
        latent_rows = lax.dynamic_slice_in_dim(latent_piece, offset, step_rows, 0)
        rotary_rows = lax.dynamic_slice_in_dim(rotary_piece, offset, step_rows, 0)
        return lax.cond(
            offset <= last_query,
            lambda carried: attend(carried, latent_rows, rotary_rows, offset),
            lambda carried: carried,
            inner_state,
        )

    running, total_sum, summed = lax.fori_loop(0, piece_rows // step_rows, one_step, initial)
    attention = (
        (summed / total_sum[..., None])
        .transpose(1, 0, 2)
        .reshape(local_rows, heads_here * VALUE_DIM)
    )
    attention = attention.astype(jnp.bfloat16)
    projected = sum_at_owner(
        jnp.dot(attention, out_proj, preferred_element_type=jnp.float32).astype(jnp.bfloat16),
        "tp",
        0,
    )
    mixed = (resid.astype(jnp.float32) + rms_scale(projected, attn_gain)).astype(jnp.bfloat16)
    normed = rms_scale(mixed.astype(jnp.float32), pre_gain).astype(jnp.bfloat16)
    rows_here = resid.shape[0]
    tp_count = lax.axis_size("tp")
    experts = lax.axis_size("sp")
    capacity = max(2, 2 * rows_here * TOP_K // experts)
    own_table, target = dispatch_table(normed, routes, experts, capacity)
    arrived = lax.all_to_all(own_table, "sp", split_axis=0, concat_axis=0, tiled=True)
    column = lax.all_gather(arrived[None], "tp", axis=0, tiled=True)
    group_normed = lax.all_gather(normed, "tp", axis=0, tiled=True)
    expert_out = expert_block(
        column.reshape(-1, MODEL_DIM), expert_gate[0], expert_up[0], expert_down[0]
    )
    shared_part = expert_block(group_normed, shared_gate, shared_up, shared_down)
    routed_sum, shared_sum = (
        lax.psum_scatter(
            expert_out.reshape(column.shape).astype(jnp.float32).astype(jnp.bfloat16),
            "tp",
            scatter_dimension=0,
            tiled=True,
        ).astype(jnp.float32),
        lax.psum_scatter(
            shared_part.reshape(tp_count, rows_here, MODEL_DIM)
            .astype(jnp.float32)
            .astype(jnp.bfloat16),
            "tp",
            scatter_dimension=0,
            tiled=True,
        ).astype(jnp.float32),
    )
    expert_rows = lax.all_to_all(
        routed_sum.astype(jnp.bfloat16), "sp", split_axis=1, concat_axis=1, tiled=True
    ).reshape(-1, MODEL_DIM)
    shared_out = shared_sum.reshape(rows_here, MODEL_DIM)
    picked = expert_rows[target].astype(jnp.float32).reshape(rows_here, TOP_K, MODEL_DIM)
    routed = jnp.sum(picked * route_weights[..., None], axis=1)
    moe = shared_out + routed
    return (mixed.astype(jnp.float32) + rms_scale(moe, moe_gain)).astype(jnp.bfloat16)


def solution(mesh):
    in_specs = (
        P("sp", "tp"),
        P("sp", "tp"),
        P("sp", None),
        P("sp", None),
        P(),
        P(None, "tp"),
        P(None, "tp"),
        P("tp", None),
        P(("sp", "tp"), None),
        P(),
        P(),
        P(("sp", "tp"), None),
        P(("sp", "tp"), None),
        P("sp", None, "tp"),
        P("sp", None, "tp"),
        P("sp", "tp", None),
        P(None, "tp"),
        P(None, "tp"),
        P("tp", None),
        P(),
    )
    out_specs = P(("sp", "tp"), None)
    return jax.shard_map(
        on_device, mesh=mesh, in_specs=in_specs, out_specs=out_specs, check_vma=False
    )
```

profile of v0, /device:TPU:0, one launch (start us, length us, event | category | flops | bytes accessed | tf_op | source)
XLA Modules:
  0.0 656.6 jit_solution(17741494576442215457)
XLA Ops:
  6.5 1.2 fusion.42
  7.8 1.7 fusion.44
  9.5 0.7 convert_element_type.118
  10.2 1.1 copy.62
  11.3 0.7 multiply_cosine_fusion
  12.1 26.5 %all-gather.1 = bf16[32,192,32]{1,2,0:T(8,128)(2,1)S(1)} all-gather(bf16[1,192,32]{1,2,0:T(8,128)(2,1)S(1)} %maximum_bitcast_fusion), channel_id=1, replica_groups=mesh['sp'=32,'tp'=4] {'sp'}, dimensions={0}, use_global_device_ids=true | all-gather | bytes 405504 | tf_op jit(solution)/shard_map/all_gather | solution.py:153
  38.9 1.3 reshape.267
  40.2 1.0 copy.60
  41.2 0.8 subtract_convert_fusion
  42.0 19.7 %all-gather.6.cloned.1.call-done = bf16[6144,512]{1,0:T(8,128)(2,1)} async-done(((bf16[192,512]{1,0:T(8,128)(2,1)}), bf16[6144,512]{1,0:T(8,128)(2,1)}) %all-gather.6.cloned.1.call-update) | async-done | bytes 6291472 | tf_op jit(solution)/shard_map/all_gather | solution.py:152
  61.7 1.1 broadcast_in_dim.34
  62.9 22.6 %while.18 = (s32[]{:T(128)}, f32[16,192]{1,0:T(8,128)S(1)}, f32[16,192]{1,0:T(8,128)S(1)}, f32[16,192,64]{1,2,0:T(8,128)}, s32[]{:T(128)}, /*index=5*/bf16[6144,...) while((s32[]{:T(128)}, f32[16,192]{1,0:T(8,128)S(1)}, ...), condition=%wide.region_6.7_spmd.clone, body=%wide.region_1.6_spmd.clone.sunk | while | flops 1591188224 | bytes 74948008 | solution.py:168
  62.9 22.1 %conditional.3 = ((f32[16,192]{1,0:T(8,128)S(1)}, f32[16,192]{1,0:T(8,128)S(1)}, f32[16,192,64]{1,2,0:T(8,128)})) conditional(s32[]{:T(128)} %convert_element_type.188, (f32[16,192]{1,0:T(8,128)S(1)}, f32[16,192]{1,0:T(8,128)S(1)}, f32[16,192,64]{1,2,0:T(8,128)}) %tuple.60, (s32[]{:T(128)}, s32[]{:T(128)}, bf16[6144,512]{1,0:T(8,128)(2,1)}, ...), branch_computations={%region_2.0_spmd, %region_3.5_spmd} | conditional | flops 1591188224 | bytes 74946960 | solution.py:161
  62.9 3.2 convolution_convert_fusion.1
  66.1 1.5 copy.58
  67.6 2.1 fusion.59
  69.8 2.9 fusion.58
  72.7 1.6 fusion.5
  74.3 1.0 copy-done.1
  75.4 2.8 convolution_convert_fusion
  78.1 1.5 copy.59
  79.6 5.4 fusion.9
  85.5 1.3 divide_convert_fusion
  86.8 6.4 convolution_convert_fusion.5
  93.2 4.5 all-to-all-start
  98.9 20.2 %all-to-all-done = bf16[4,48,4096]{2,1,0:T(8,128)(2,1)} async-done(((bf16[4,48,4096]{2,1,0:T(8,128)(2,1)}), bf16[4,48,4096]{2,1,0:T(8,128)(2,1)}, u32[]{:S(2)}, u32[]{:S(2)}) %all-to-all-start) | async-done | bytes 1572896 | tf_op jit(solution)/shard_map/all_to_all | solution.py:26
  119.1 1.7 convert_reduce_fusion
  121.6 1.8 convolution_convert_fusion.3
  123.4 3.5 reshape.247
  126.9 275.5 %all_to_all.15 = bf16[32,6,4096]{2,1,0:T(8,128)(2,1)S(1)} all-to-all(bf16[32,6,4096]{2,1,0:T(8,128)(2,1)} %reshape.247), channel_id=1, replica_groups=mesh['sp'=32,'tp'=4] {'sp'}, dimensions={0} | all-to-all | bytes 3145728 | tf_op jit(solution)/shard_map/all_to_all | solution.py:187
  402.3 2.1 copy.66
  405.2 60.8 %all-gather.10.cloned.1.call-done = bf16[128,6,4096]{2,0,1:T(8,128)(2,1)} async-done(((bf16[32,6,4096]{2,0,1:T(8,128)(2,1)}), bf16[128,6,4096]{2,0,1:T(8,128)(2,1)}) %all-gather.10.cloned.1.call-update) | async-done | bytes 6291472 | tf_op jit(solution)/shard_map/all_gather | solution.py:188
  466.1 9.6 %copy.67 = bf16[128,6,4096]{2,1,0:T(8,128)(2,1)} copy(bf16[128,6,4096]{2,0,1:T(8,128)(2,1)} %all-gather.10.cloned.1.call-done) | data formatting | bytes 12582912 | tf_op jit(solution)/shard_map/all_gather | solution.py:188
  475.6 10.3 %reshape.248 = bf16[768,4096]{1,0:T(8,128)(2,1)} reshape(bf16[128,6,4096]{2,1,0:T(8,128)(2,1)} %copy.67) | data formatting | bytes 12582912 | tf_op jit(solution)/shard_map/reshape | solution.py:191
  486.0 6.2 fusion.22
  492.2 12.8 %convolution_convert_fusion.2 = bf16[768,4096]{1,0:T(8,128)(2,1)} fusion(bf16[1,256,4096]{2,1,0:T(8,128)(2,1)S(1)} %copy-done, bf16[768,4096]{1,0:T(8,128)(2,1)} %reshape.248, bf16[1,4096,256]{2,1,0:T(8,128)(2,1)} %param.38, f32[768,256]{1,0:T(8,128)} %fusion.22), kind=kOutput, calls=%fused_computation.25 | convolution fusion | flops 3225550848 | bytes 17563648 | tf_op jit(solution)/shard_map/dot_general | solution.py:60
  505.0 10.1 %reshape.249 = bf16[4,32,6,4096]{3,2,1,0:T(8,128)(2,1)} reshape(bf16[768,4096]{1,0:T(8,128)(2,1)} %convolution_convert_fusion.2) | data formatting | bytes 12582912 | tf_op jit(solution)/shard_map/reshape | solution.py:196
  515.4 2.6 fusion.60
  518.1 5.7 convolution_convert_fusion.4
  523.8 72.6 %reduce-scatter.5.cloned.1.call-done = bf16[1,32,6,4096]{3,2,1,0:T(8,128)(2,1)} async-done(((bf16[4,32,6,4096]{3,2,1,0:T(8,128)(2,1)}), bf16[1,32,6,4096]{3,2,1,0:T(8,128)(2,1)}) %reduce-scatter.5.cloned.1.call-update) | async-done | bytes 1572880 | tf_op jit(solution)/shard_map/reduce_scatter | solution.py:195
  596.5 7.5 %all-to-all-start.2 = ((bf16[1,32,6,4096]{3,2,0,1:T(8,128)(2,1)}), bf16[1,32,6,4096]{3,2,0,1:T(8,128)(2,1)}, u32[]{:S(2)}, u32[]{:S(2)}) async-start(bf16[1,32,6,4096]{3,2,0,1:T(8,128)(2,1)} %bitcast.77), calls=%async_computation.4 | async-start | bytes 4194304 | tf_op jit(solution)/shard_map/all_to_all | solution.py:210
  604.2 29.8 %all-to-all-done.2 = bf16[1,32,6,4096]{3,2,0,1:T(8,128)(2,1)} async-done(((bf16[1,32,6,4096]{3,2,0,1:T(8,128)(2,1)}), bf16[1,32,6,4096]{3,2,0,1:T(8,128)(2,1)}, u32[]{:S(2)}, u32[]{:S(2)}) %all-to-all-start.2) | async-done | bytes 1572896 | tf_op jit(solution)/shard_map/all_to_all | solution.py:210
  634.0 3.7 reshape.250
  637.7 3.4 gather_fusion
  641.1 2.1 reshape.255
  643.2 3.6 multiply_reduce_fusion
  646.9 1.2 multiply_reduce_fusion.1
  648.1 1.9 fusion.36
  (89 shorter events, 3.9 us)
Async XLA Ops:
  6.5 485.7 %copy-start = (bf16[1,256,4096]{2,1,0:T(8,128)(2,1)S(1)}, bf16[1,256,4096]{2,1,0:T(8,128)(2,1)}, u32[]{:S(2)}) copy-start(bf16[1,256,4096]{2,1,0:T(8,128)(2,1)} %param.39) | copy-start | bytes 6291460
  6.5 33.6 %copy-start.3 = (bf16[192,1024]{1,0:T(8,128)(2,1)S(1)}, bf16[192,1024]{1,0:T(8,128)(2,1)}, u32[]{:S(2)}) copy-start(bf16[192,1024]{1,0:T(8,128)(2,1)} %param.24) | copy-start | bytes 1179652
  6.5 55.2 %all-gather.6.cloned.1.call-start = ((), (), s32[]{:S(2)}) async-start(), calls=%async_computation.5 | async-start | bytes 6488064 | tf_op jit(solution)/shard_map/all_gather | solution.py:152
  72.6 2.7 copy-start.1
  72.7 2.7 copy-start.10
  93.2 4.7 copy-start.8
  93.2 25.9 %all-to-all-start = ((bf16[4,48,4096]{2,1,0:T(8,128)(2,1)}), bf16[4,48,4096]{2,1,0:T(8,128)(2,1)}, u32[]{:S(2)}, u32[]{:S(2)}) async-start(bf16[4,48,4096]{2,1,0:T(8,128)(2,1)} %bitcast.75), calls=%async_computation | async-start | bytes 3145728 | tf_op jit(solution)/shard_map/all_to_all | solution.py:26
  97.7 23.4 %copy-start.4 = (bf16[48,4096]{1,0:T(8,128)(2,1)S(1)}, bf16[48,4096]{1,0:T(8,128)(2,1)}, u32[]{:S(2)}) copy-start(bf16[48,4096]{1,0:T(8,128)(2,1)} %param.32) | copy-start | bytes 1179652
  97.7 23.4 %copy-start.5 = (f32[4096]{0:T(1024)S(1)}, f32[4096]{0:T(1024)}, u32[]{:S(2)}) copy-start(f32[4096]{0:T(1024)} %param.33) | copy-start | bytes 49156
  97.7 368.4 %all-gather.10.cloned.1.call-start = ((), (), s32[]{:S(2)}) async-start(), calls=%async_computation.9 | async-start | bytes 7864320 | tf_op jit(solution)/shard_map/all_gather | solution.py:188
  98.9 22.5 %copy-start.7 = (f32[4096]{0:T(1024)S(1)}, f32[4096]{0:T(1024)}, u32[]{:S(2)}) copy-start(f32[4096]{0:T(1024)} %param.34) | copy-start | bytes 49156
  121.6 5.3 copy-start.2
  404.5 111.0 %all-gather.8.cloned.1.call-start = ((), (), s32[]{:S(2)}) async-start(), calls=%async_computation.6 | async-start | bytes 1966080 | tf_op jit(solution)/shard_map/all_gather | solution.py:189
  405.2 191.3 %reduce-scatter.5.cloned.1.call-start = ((), (), s32[]{:S(2)}) async-start(), calls=%async_computation.8 | async-start | bytes 10485760 | tf_op jit(solution)/shard_map/reduce_scatter | solution.py:195
  515.1 131.7 %reduce-scatter.3.cloned.1.call-start = ((), (), s32[]{:S(2)}) async-start(), calls=%async_computation.7 | async-start | bytes 1966080 | tf_op jit(solution)/shard_map/reduce_scatter | solution.py:201
  596.5 7.6 %copy-start.9 = (f32[48,2]{0,1:T(2,128)S(1)}, f32[48,2]{0,1:T(2,128)}, u32[]{:S(2)}) copy-start(f32[48,2]{0,1:T(2,128)} %param.36) | copy-start | bytes 1156
  596.5 37.6 %all-to-all-start.2 = ((bf16[1,32,6,4096]{3,2,0,1:T(8,128)(2,1)}), bf16[1,32,6,4096]{3,2,0,1:T(8,128)(2,1)}, u32[]{:S(2)}, u32[]{:S(2)}) async-start(bf16[1,32,6,4096]{3,2,0,1:T(8,128)(2,1)} %bitcast.77), calls=%async_computation.4 | async-start | bytes 4194304 | tf_op jit(solution)/shard_map/all_to_all | solution.py:210
  643.2 4.9 copy-start.6
Sparse Core Ops, SparseCore 0:
  9.6 52.0 all-gather.5
  404.6 61.4 all-gather.9
  467.8 27.0 all-gather.7
  515.3 81.1 reduce-scatter.4
  598.7 25.3 reduce-scatter.2
where the time goes:
time: 661 us; the launch traced here: 657 us
  blocking collectives  302 us (46%)
  waiting for transfers between devices  204 us (31%)
  local copies, waits for them, and re-layouts  54.2 us (8%)
  matrix products  51.7 us (8%)
  other arithmetic  18.1 us (3%)
  between operations  13.4 us (2%)
  starting transfers between devices  12.5 us (2%)
    all_to_all x1, blocking collectives, on_device(): lax.all_to_all(own_table, 'sp', split_axis=0, concat_axis=0, tiled=True)  275 us
    reduce_scatter x1, waiting for transfers between devices, on_device(): lax.psum_scatter(expert_out.reshape(column.shape).astype(jnp.float32).ast...  72.6 us
    all_gather x1, waiting for transfers between devices, on_device(): column = lax.all_gather(arrived[None], 'tp', axis=0, tiled=True)  60.8 us
    all_to_all x1, waiting for transfers between devices, on_device(): lax.all_to_all(routed_sum.astype(jnp.bfloat16), 'sp', split_axis=1, conca...  29.8 us
    all_gather x1, blocking collectives, on_device(): rotary_piece = lax.all_gather(key_rot, 'sp', axis=0, tiled=True)  26.5 us
    all_to_all x1, waiting for transfers between devices, sum_at_owner(): lax.all_to_all(cut_along(array, dim, count), axis, 0, 0, tiled=True)  20.2 us
    all_gather x1, waiting for transfers between devices, on_device(): latent_piece = lax.all_gather(latent_normed, 'sp', axis=0, tiled=True)  19.7 us
    dot_general x2, matrix products, expert_block(): jnp.dot(hidden, down_part, preferred_element_type=jnp.float32)  18.5 us
  transfers between devices with their start and end apart: 7, of which 5 were waited for; matrix products, arithmetic and copies ran while one was open for 12% of the time, Pallas kernels for 0%

commit v1 on v0

--- a/solution.py
+++ b/solution.py
@@ -1,8 +1,11 @@
+import functools
 import math
 
 import jax
 import jax.numpy as jnp
 from jax import lax
+from jax.experimental import pallas as pl
+from jax.experimental.pallas import tpu as pltpu
 from jax.sharding import PartitionSpec as P
 
 MODEL_DIM = 4096
@@ -77,6 +80,131 @@
         jnp.bfloat16
     )
     return (slot_table.reshape(experts, capacity, normed_rows.shape[1]), target)
+
+
+BLK = 1024
+
+def attend_kernel(index_fn, lat_ref, qn_ref, qr_ref, wk_ref, wv_ref, out_ref, kcat, vcat, qs, acc, mx, sa, sb):
+    rows = qn_ref.shape[0]
+    pairs = qn_ref.shape[1] // 128
+    s = index_fn()
+    nkeys = (s + 1) * rows
+    steps = (nkeys + 2 * BLK - 1) // (2 * BLK)
+    free = (s * rows) // (2 * BLK)
+    c = (96 ** -0.5) * math.log2(math.e)
+
+    def at(i):
+        return pl.ds(pl.multiple_of(i * BLK, BLK), BLK)
+
+    def prep(i, _):
+        for par in range(2):
+            kcat[par, at(i), 128:256] = lat_ref[at(i), 512:640]
+            vcat[par, at(i), 128:256] = jnp.ones((BLK, 128), jnp.bfloat16)
+        return 0
+
+    lax.fori_loop(0, 2 * steps, prep, 0)
+    lane = lax.broadcasted_iota(jnp.int32, (rows, 128), 1)
+
+    def weights(j):
+        cols = pl.ds(pl.multiple_of(j * 128, 128), 128)
+        return jnp.concatenate([wk_ref[:, cols], wv_ref[:, cols]], axis=1)
+
+    w0 = weights(0)
+
+    def up0(i, _):
+        kv = jnp.dot(lat_ref[at(i), 0:512], w0, preferred_element_type=jnp.float32).astype(jnp.bfloat16)
+        kcat[0, at(i), 0:128] = kv[:, 0:128]
+        vcat[0, at(i), 0:128] = kv[:, 128:256]
+        return 0
+
+    lax.fori_loop(0, 2 * steps, up0, 0)
+
+    def one_pair(j, _):
+        par = j % 2
+        cols = pl.ds(pl.multiple_of(j * 128, 128), 128)
+        qp = qn_ref[:, cols]
+        zero = jnp.zeros_like(qp)
+        g = qr_ref[:, pl.ds(pl.multiple_of((j // 2) * 128, 128), 128)]
+        first = 2 * (j % 2)
+        qs[0:rows, 0:128] = jnp.where(lane < 64, qp, zero)
+        qs[rows:, 0:128] = jnp.where(lane >= 64, qp, zero)
+        qs[0:rows, 128:256] = jnp.where(lane // 32 == first, g, zero)
+        qs[rows:, 128:256] = jnp.where(lane // 32 == first + 1, g, zero)
+        nxt = jnp.minimum(j + 1, pairs - 1)
+        ncols = pl.ds(pl.multiple_of(nxt * 128, 128), 128)
+        acc[...] = jnp.zeros_like(acc)
+        mx[...] = jnp.full_like(mx, -1e30)
+
+        def scores(i):
+            return lax.dot_general(qs[...], kcat[par, at(i), :], (((1,), (1,)), ((), ())), preferred_element_type=jnp.float32)
+
+        sa[...] = scores(0)
+
+        def block(i, cur, other, masked):
+            vb = vcat[par, at(i), :]
+            w = jnp.concatenate([wk_ref[:, ncols], wv_ref[:, ncols]], axis=1)
+            kv = jnp.dot(lat_ref[at(i), 0:512], w, preferred_element_type=jnp.float32).astype(jnp.bfloat16)
+            snext = scores(jnp.minimum(i + 1, 2 * steps - 1))
+            for half in range(2):
+                rs = pl.ds(half * rows, rows)
+                sc = cur[rs, :]
+                if masked:
+                    qpos = s * rows + lax.broadcasted_iota(jnp.int32, (rows, BLK), 0)
+                    kpos = i * BLK + lax.broadcasted_iota(jnp.int32, (rows, BLK), 1)
+                    sc = jnp.where(kpos <= qpos, sc, -1e30)
+                old = mx[rs, :]
+                new = jnp.maximum(old, jnp.max(sc, axis=1, keepdims=True))
+                newc = new * c
+                p = jnp.concatenate([jnp.exp2(sc[:, k * 128:(k + 1) * 128] * c - newc).astype(jnp.bfloat16) for k in range(BLK // 128)], axis=1)
+                factor = jnp.exp2(old * c - newc)
+                mx[rs, :] = new
+                pv = jnp.dot(p, vb, preferred_element_type=jnp.float32)
+                acc[rs, 0:128] = acc[rs, 0:128] * factor + pv[:, 0:128]
+                acc[rs, 128:256] = acc[rs, 128:256] * factor + pv[:, 128:256]
+            other[...] = snext
+            kcat[1 - par, at(i), 0:128] = kv[:, 0:128]
+            vcat[1 - par, at(i), 0:128] = kv[:, 128:256]
+
+        def plain(i, _):
+            block(2 * i, sa, sb, False)
+            block(2 * i + 1, sb, sa, False)
+            return 0
+
+        def edge(i, _):
+            block(2 * i, sa, sb, True)
+            block(2 * i + 1, sb, sa, True)
+            return 0
+
+        lax.fori_loop(0, free, plain, 0)
+        lax.fori_loop(free, steps, edge, 0)
+        o0 = acc[0:rows, 0:128] / acc[0:rows, 128:256]
+        o1 = acc[rows:, 0:128] / acc[rows:, 128:256]
+        out_ref[:, cols] = jnp.where(lane < 64, o0, o1).astype(jnp.bfloat16)
+        return 0
+
+    lax.fori_loop(0, pairs, one_pair, 0)
+
+
+def attend(index_fn, lat, qn, qr, wk, wv):
+    rows = qn.shape[0]
+    keys = lat.shape[0]
+    return pl.pallas_call(
+        functools.partial(attend_kernel, index_fn),
+        out_shape=jax.ShapeDtypeStruct(qn.shape, jnp.bfloat16),
+        in_specs=[pl.BlockSpec(memory_space=pltpu.VMEM)] * 5,
+        out_specs=pl.BlockSpec(memory_space=pltpu.VMEM),
+        scratch_shapes=[
+            pltpu.VMEM((2, keys, 256), jnp.bfloat16),
+            pltpu.VMEM((2, keys, 256), jnp.bfloat16),
+            pltpu.VMEM((2 * rows, 256), jnp.bfloat16),
+            pltpu.VMEM((2 * rows, 256), jnp.float32),
+            pltpu.VMEM((2 * rows, 128), jnp.float32),
+            pltpu.VMEM((2 * rows, BLK), jnp.float32),
+            pltpu.VMEM((2 * rows, BLK), jnp.float32),
+        ],
+        compiler_params=pltpu.CompilerParams(vmem_limit_bytes=48 * 1024 * 1024),
+        name="attend",
+    )(lat, qn, qr, wk, wv)
 
 
 def on_device(
@@ -104,74 +232,22 @@
     local_rows = query_nope.shape[0]
     heads_here = query_nope.shape[1] // NOPE_DIM
     query_pos = lax.axis_index("sp") * local_rows + jnp.arange(local_rows, dtype=jnp.int32)
-    last_query = lax.axis_index("sp") * local_rows + local_rows - 1
+    key_rot = rotate(key_rope.astype(jnp.float32), query_pos).astype(jnp.bfloat16)
+    latent_normed = rms_scale(latent.astype(jnp.float32), latent_gain).astype(jnp.bfloat16)
+    latent_all = lax.all_gather(
+        jnp.concatenate([latent_normed] + [key_rot] * 4, axis=1), "sp", axis=0, tiled=True
+    )
     query_rot = rotate(
         query_rope.astype(jnp.float32).reshape(local_rows, heads_here, ROPE_DIM), query_pos[:, None]
     ).astype(jnp.bfloat16)
-    key_rot = rotate(key_rope.astype(jnp.float32), query_pos).astype(jnp.bfloat16)
-    latent_normed = rms_scale(latent.astype(jnp.float32), latent_gain).astype(jnp.bfloat16)
-    query_heads = query_nope.reshape(local_rows, heads_here, NOPE_DIM)
-    score_scale = (NOPE_DIM + ROPE_DIM) ** (-0.5)
-
-    def attend(state_now, latent_rows, rotary_rows, key_start):
-        piece_rows = latent_rows.shape[0]
-        keys_here = jnp.dot(latent_rows, key_up, preferred_element_type=jnp.float32).astype(
-            jnp.bfloat16
-        )
-        keys_here = keys_here.reshape(piece_rows, heads_here, NOPE_DIM)
-        values_here = jnp.dot(latent_rows, value_up, preferred_element_type=jnp.float32).astype(
-            jnp.bfloat16
-        )
-        values_here = values_here.reshape(piece_rows, heads_here, VALUE_DIM)
-        scores = (
-            jnp.einsum("qhd,khd->hqk", query_heads, keys_here, preferred_element_type=jnp.float32)
-            + jnp.einsum("qhr,kr->hqk", query_rot, rotary_rows, preferred_element_type=jnp.float32)
-        ) * score_scale
-        allowed = (key_start + jnp.arange(piece_rows, dtype=jnp.int32))[None, :] <= query_pos[
-            :, None
-        ]
-        scores = jnp.where(allowed[None], scores, -1e30)
-        running, total_sum, summed = state_now
-        newest = jnp.maximum(running, jnp.max(scores, axis=-1))
-        factor = jnp.exp(running - newest)
-        exponent = jnp.exp(scores - newest[..., None])
-        total_sum = total_sum * factor + jnp.sum(exponent, axis=-1)
-        summed = summed * factor[..., None] + jnp.einsum(
-            "hqk,khd->hqd",
-            exponent.astype(jnp.bfloat16),
-            values_here,
-            preferred_element_type=jnp.float32,
-        )
-        return (newest, total_sum, summed)
-
-    initial = (
-        jnp.full((heads_here, local_rows), -1e30, jnp.float32),
-        jnp.zeros((heads_here, local_rows), jnp.float32),
-        jnp.zeros((heads_here, local_rows, VALUE_DIM), jnp.float32),
-    )
-    latent_piece = lax.all_gather(latent_normed, "sp", axis=0, tiled=True)
-    rotary_piece = lax.all_gather(key_rot, "sp", axis=0, tiled=True)
-    piece_rows = latent_piece.shape[0]
-    step_rows = math.gcd(piece_rows, 512)
-
-    def one_step(step_index, inner_state):
-        offset = step_index * step_rows
-        latent_rows = lax.dynamic_slice_in_dim(latent_piece, offset, step_rows, 0)
-        rotary_rows = lax.dynamic_slice_in_dim(rotary_piece, offset, step_rows, 0)
-        return lax.cond(
-            offset <= last_query,
-            lambda carried: attend(carried, latent_rows, rotary_rows, offset),
-            lambda carried: carried,
-            inner_state,
-        )
-
-    running, total_sum, summed = lax.fori_loop(0, piece_rows // step_rows, one_step, initial)
-    attention = (
-        (summed / total_sum[..., None])
-        .transpose(1, 0, 2)
-        .reshape(local_rows, heads_here * VALUE_DIM)
-    )
-    attention = attention.astype(jnp.bfloat16)
+    attention = attend(
+        lambda: lax.axis_index("sp"),
+        latent_all,
+        query_nope,
+        query_rot.reshape(local_rows, -1),
+        key_up,
+        value_up,
+    )
     projected = sum_at_owner(
         jnp.dot(attention, out_proj, preferred_element_type=jnp.float32).astype(jnp.bfloat16),
         "tp",

time: 661 us -> 447 us (0.68)
  blocking collectives: 302 us -> 65.3 us
  waiting for transfers between devices: 204 us -> 235 us
  Pallas kernels: 0 us -> 24.1 us
  matrix products: 51.7 us -> 31.7 us
    all_to_all x1, blocking collectives: 275 us -> 65.3 us  [on_device(): lax.all_to_all(own_table, 'sp', split_axis=0, concat_axis=0, tiled=True)]
    all_gather x1, waiting for transfers between devices: 19.7 us -> 50.4 us  [on_device(): lax.all_gather(jnp.concatenate([latent_normed] + [key_rot] * 4, axis=1),...]
    all_gather x1 -> x0, blocking collectives: 26.5 us -> none  [on_device(): rotary_piece = lax.all_gather(key_rot, 'sp', axis=0, tiled=True)]
    pallas_call x0 -> x1, Pallas kernels: none -> 24.1 us  [attend(): pl.pallas_call(functools.partial(attend_kernel, index_fn), out_shape=jax....]
    dot_general x5 -> x0, matrix products: 16.2 us -> none  [the longest x1 5.36 us: attend(): jnp.einsum('hqk,khd->hqd', exponent.astype(jnp.bfloat16), values_here, pr...]
  transfers between devices with their start and end apart: 7 -> 7, of which waited for: 5 -> 5; matrix products, arithmetic and copies ran while one was open for 12% -> 16% of each run, Pallas kernels for 0% -> 0%
where the time goes in v1:
time: 447 us; the launch traced here: 445 us
  waiting for transfers between devices  235 us (53%)
  blocking collectives  65.3 us (15%)
  local copies, waits for them, and re-layouts  49.2 us (11%)
  matrix products  31.7 us (7%)
  Pallas kernels  24.1 us (5%)
  other arithmetic  14 us (3%)
  between operations  13.4 us (3%)
  starting transfers between devices  12.6 us (3%)
    reduce_scatter x1, waiting for transfers between devices, on_device(): lax.psum_scatter(expert_out.reshape(column.shape).astype(jnp.float32).ast...  73 us
    all_to_all x1, blocking collectives, on_device(): lax.all_to_all(own_table, 'sp', split_axis=0, concat_axis=0, tiled=True)  65.3 us
    all_gather x1, waiting for transfers between devices, on_device(): column = lax.all_gather(arrived[None], 'tp', axis=0, tiled=True)  60.7 us
    all_gather x1, waiting for transfers between devices, on_device(): lax.all_gather(jnp.concatenate([latent_normed] + [key_rot] * 4, axis=1),...  50.4 us
    all_to_all x1, waiting for transfers between devices, on_device(): lax.all_to_all(routed_sum.astype(jnp.bfloat16), 'sp', split_axis=1, conca...  29.8 us
    pallas_call x1, Pallas kernels, attend(): pl.pallas_call(functools.partial(attend_kernel, index_fn), out_shape=jax....  24.1 us
    all_to_all x1, waiting for transfers between devices, sum_at_owner(): lax.all_to_all(cut_along(array, dim, count), axis, 0, 0, tiled=True)  20.4 us
    dot_general x2, matrix products, expert_block(): jnp.dot(hidden, down_part, preferred_element_type=jnp.float32)  18 us
  transfers between devices with their start and end apart: 7, of which 5 were waited for; matrix products, arithmetic and copies ran while one was open for 16% of the time, Pallas kernels for 0%

profile of v1, /device:TPU:0, one launch (start us, length us, event | category | flops | bytes accessed | tf_op | source)
XLA Modules:
  0.0 445.2 jit_solution(12884976663832303039)
XLA Ops:
  6.6 1.0 copy.56
  7.6 1.0 fusion.23
  8.6 1.0 fusion.25
  9.7 1.1 multiply_cosine_fusion
  10.8 0.9 concatenate.10
  11.7 1.0 copy.59
  12.7 1.1 copy.58
  13.9 0.7 pad_maximum_fusion
  14.7 1.1 copy.61.qr_ref
  15.7 50.4 %all-gather.5.cloned.1.call-done.lat_ref = bf16[6144,640]{1,0:T(8,128)(2,1)} async-done(((bf16[192,640]{1,0:T(8,128)(2,1)}), bf16[6144,640]{1,0:T(8,128)(2,1)}) %all-gather.5.cloned.1.call-update) | async-done | bytes 7864336 | tf_op jit(solution)/shard_map/all_gather | solution.py:237
  66.1 1.2 copy-done.3
  67.4 1.0 copy-done.4
  68.4 24.1 %attend.1 = bf16[192,1024]{1,0:T(8,128)(2,1)S(1)} custom-call(bf16[6144,640]{1,0:T(8,128)(2,1)} %all-gather.5.cloned.1.call-done.lat_ref, bf16[192,1024]{1,0:T(8,128)(2,1)S(1)} %copy-done.4, bf16[192,512]{1,0:T(8,128)(2,1)S(1)} %copy.61.qr_ref, bf16[512,1024]{1,0:T(8,128)(2,1)S(1)} %copy-done.2, bf16[512,1024]{1,0:T(8,128)(2,1)S(1)} %copy-done.3), custom_call_target="tpu_custom_call" | custom-call | tf_op jit(solution)/shard_map/attend/pallas_call | solution.py:191
  92.5 3.0 convolution_convert_fusion.3
  95.4 4.5 %all-to-all-start = ((bf16[4,48,4096]{2,1,0:T(8,128)(2,1)}), bf16[4,48,4096]{2,1,0:T(8,128)(2,1)}, u32[]{:S(2)}, u32[]{:S(2)}) async-start(bf16[4,48,4096]{2,1,0:T(8,128)(2,1)} %bitcast.46), calls=%async_computation | async-start | bytes 3145728 | tf_op jit(solution)/shard_map/all_to_all | solution.py:29
  100.1 0.1 eq.28
  100.3 0.1 reduce_window_sum.11
  100.4 0.2 select_reduce_fusion
  100.6 0.1 reduce_sum.72
  100.9 20.4 %all-to-all-done = bf16[4,48,4096]{2,1,0:T(8,128)(2,1)} async-done(((bf16[4,48,4096]{2,1,0:T(8,128)(2,1)}), bf16[4,48,4096]{2,1,0:T(8,128)(2,1)}, u32[]{:S(2)}, u32[]{:S(2)}) %all-to-all-start) | async-done | bytes 1572896 | tf_op jit(solution)/shard_map/all_to_all | solution.py:29
  121.4 1.7 convert_reduce_fusion
  123.1 0.2 multiply_reduce_fusion.2
  123.3 0.4 fusion.14
  123.7 0.2 fusion.16
  123.8 1.8 convolution_convert_fusion.1
  125.6 3.5 reshape.198
  129.1 65.3 %all_to_all.15 = bf16[32,6,4096]{2,1,0:T(8,128)(2,1)S(1)} all-to-all(bf16[32,6,4096]{2,1,0:T(8,128)(2,1)} %reshape.198), channel_id=1, replica_groups=mesh['sp'=32,'tp'=4] {'sp'}, dimensions={0} | all-to-all | bytes 3145728 | tf_op jit(solution)/shard_map/all_to_all | solution.py:263
  194.3 2.1 copy.65
  196.5 0.7 all-gather.7.cloned.1.call-update
  197.2 0.2 reduce-scatter.5.cloned.1.call-start
  197.4 60.7 %all-gather.9.cloned.1.call-done = bf16[128,6,4096]{2,0,1:T(8,128)(2,1)} async-done(((bf16[32,6,4096]{2,0,1:T(8,128)(2,1)}), bf16[128,6,4096]{2,0,1:T(8,128)(2,1)}) %all-gather.9.cloned.1.call-update) | async-done | bytes 6291472 | tf_op jit(solution)/shard_map/all_gather | solution.py:264
  258.1 9.6 %copy.66 = bf16[128,6,4096]{2,1,0:T(8,128)(2,1)} copy(bf16[128,6,4096]{2,0,1:T(8,128)(2,1)} %all-gather.9.cloned.1.call-done) | data formatting | bytes 12582912 | tf_op jit(solution)/shard_map/all_gather | solution.py:264
  267.6 10.3 %reshape.199 = bf16[768,4096]{1,0:T(8,128)(2,1)} reshape(bf16[128,6,4096]{2,1,0:T(8,128)(2,1)} %copy.66) | data formatting | bytes 12582912 | tf_op jit(solution)/shard_map/reshape | solution.py:267
  277.9 6.2 %fusion.3 = f32[768,256]{1,0:T(8,128)} fusion(bf16[768,4096]{1,0:T(8,128)(2,1)} %reshape.199, bf16[1,4096,256]{2,1,0:T(8,128)(2,1)} %param.33), kind=kOutput, calls=%fused_computation.9 | convolution fusion | flops 1610612736 | bytes 9175040 | tf_op jit(solution)/shard_map/dot_general | solution.py:60
  284.2 12.7 %convolution_convert_fusion = bf16[768,4096]{1,0:T(8,128)(2,1)} fusion(bf16[1,256,4096]{2,1,0:T(8,128)(2,1)S(1)} %copy-done, bf16[768,4096]{1,0:T(8,128)(2,1)} %reshape.199, bf16[1,4096,256]{2,1,0:T(8,128)(2,1)} %param.34, f32[768,256]{1,0:T(8,128)} %fusion.3), kind=kOutput, calls=%fused_computation.1 | convolution fusion | flops 3225550848 | bytes 17563648 | tf_op jit(solution)/shard_map/dot_general | solution.py:63
  296.9 10.1 %reshape.200 = bf16[4,32,6,4096]{3,2,1,0:T(8,128)(2,1)} reshape(bf16[768,4096]{1,0:T(8,128)(2,1)} %convolution_convert_fusion) | data formatting | bytes 12582912 | tf_op jit(solution)/shard_map/reshape | solution.py:272
  307.1 0.3 reduce-scatter.3.cloned.1.call-start
  307.4 2.8 fusion.39
  310.1 5.2 %convolution_convert_fusion.2 = bf16[192,4096]{1,0:T(8,128)(2,1)} fusion(bf16[256,4096]{1,0:T(8,128)(2,1)} %param.38, bf16[192,4096]{1,0:T(8,128)(2,1)S(1)} %copy-done.5, bf16[4096,256]{1,0:T(8,128)(2,1)} %param.37, f32[192,256]{1,0:T(8,128)S(1)} %fusion.39), kind=kOutput, calls=%fused_computation.3 | convolution fusion | flops 806387712 | bytes 7536640 | tf_op jit(solution)/shard_map/dot_general | solution.py:63
  315.4 73.0 %reduce-scatter.5.cloned.1.call-done = bf16[1,32,6,4096]{3,2,1,0:T(8,128)(2,1)} async-done(((bf16[4,32,6,4096]{3,2,1,0:T(8,128)(2,1)}), bf16[1,32,6,4096]{3,2,1,0:T(8,128)(2,1)}) %reduce-scatter.5.cloned.1.call-update) | async-done | bytes 1572880 | tf_op jit(solution)/shard_map/reduce_scatter | solution.py:271
  388.4 7.5 %all-to-all-start.2 = ((bf16[1,32,6,4096]{3,2,0,1:T(8,128)(2,1)}), bf16[1,32,6,4096]{3,2,0,1:T(8,128)(2,1)}, u32[]{:S(2)}, u32[]{:S(2)}) async-start(bf16[1,32,6,4096]{3,2,0,1:T(8,128)(2,1)} %bitcast.45), calls=%async_computation.4 | async-start | bytes 4194304 | tf_op jit(solution)/shard_map/all_to_all | solution.py:286
  396.2 29.8 %all-to-all-done.2 = bf16[1,32,6,4096]{3,2,0,1:T(8,128)(2,1)} async-done(((bf16[1,32,6,4096]{3,2,0,1:T(8,128)(2,1)}), bf16[1,32,6,4096]{3,2,0,1:T(8,128)(2,1)}, u32[]{:S(2)}, u32[]{:S(2)}) %all-to-all-start.2) | async-done | bytes 1572896 | tf_op jit(solution)/shard_map/all_to_all | solution.py:286
  426.0 2.5 reshape.201
  428.5 1.0 gather_fusion
  429.6 2.1 reshape.206
  431.7 3.8 multiply_reduce_fusion
  435.5 1.2 multiply_reduce_fusion.1
  436.7 1.9 fusion.17
  (54 shorter events, 1.1 us)
Async XLA Ops:
  6.5 277.7 %copy-start = (bf16[1,256,4096]{2,1,0:T(8,128)(2,1)S(1)}, bf16[1,256,4096]{2,1,0:T(8,128)(2,1)}, u32[]{:S(2)}) copy-start(bf16[1,256,4096]{2,1,0:T(8,128)(2,1)} %param.35) | copy-start | bytes 6291460
  6.5 59.6 %all-gather.5.cloned.1.call-start = ((), (), s32[]{:S(2)}) async-start(), calls=%async_computation.5 | async-start | bytes 8110080 | tf_op jit(solution)/shard_map/all_gather | solution.py:237
  10.8 55.4 %copy-start.2 = (bf16[512,1024]{1,0:T(8,128)(2,1)S(1)}, bf16[512,1024]{1,0:T(8,128)(2,1)}, u32[]{:S(2)}) copy-start(bf16[512,1024]{1,0:T(8,128)(2,1)} %wk_ref.1) | copy-start | bytes 3145732
  66.1 1.2 copy-start.3
  67.4 1.0 copy-start.4
  68.4 24.1 %copy-start.13 = (bf16[1024,4096]{1,0:T(8,128)(2,1)S(1)}, bf16[1024,4096]{1,0:T(8,128)(2,1)}, u32[]{:S(2)}) copy-start(bf16[1024,4096]{1,0:T(8,128)(2,1)} %param.27) | copy-start | bytes 25165828
  95.4 4.6 %copy-start.11 = (s32[48,2]{0,1:T(2,128)S(1)}, s32[48,2]{0,1:T(2,128)}, u32[]{:S(2)}) copy-start(s32[48,2]{0,1:T(2,128)} %param.31) | copy-start | bytes 1156
  95.4 25.9 %all-to-all-start = ((bf16[4,48,4096]{2,1,0:T(8,128)(2,1)}), bf16[4,48,4096]{2,1,0:T(8,128)(2,1)}, u32[]{:S(2)}, u32[]{:S(2)}) async-start(bf16[4,48,4096]{2,1,0:T(8,128)(2,1)} %bitcast.46), calls=%async_computation | async-start | bytes 3145728 | tf_op jit(solution)/shard_map/all_to_all | solution.py:29
  99.9 23.4 %copy-start.7 = (bf16[48,4096]{1,0:T(8,128)(2,1)S(1)}, bf16[48,4096]{1,0:T(8,128)(2,1)}, u32[]{:S(2)}) copy-start(bf16[48,4096]{1,0:T(8,128)(2,1)} %param.28) | copy-start | bytes 1179652
  99.9 23.4 %copy-start.8 = (f32[4096]{0:T(1024)S(1)}, f32[4096]{0:T(1024)}, u32[]{:S(2)}) copy-start(f32[4096]{0:T(1024)} %param.29) | copy-start | bytes 49156
  99.9 158.2 %all-gather.9.cloned.1.call-start = ((), (), s32[]{:S(2)}) async-start(), calls=%async_computation.9 | async-start | bytes 7864320 | tf_op jit(solution)/shard_map/all_gather | solution.py:264
  100.9 22.7 %copy-start.10 = (f32[4096]{0:T(1024)S(1)}, f32[4096]{0:T(1024)}, u32[]{:S(2)}) copy-start(f32[4096]{0:T(1024)} %param.30) | copy-start | bytes 49156
  123.8 5.3 %copy-start.6 = (bf16[48,4096]{1,0:T(8,128)(2,1)}, bf16[48,4096]{1,0:T(8,128)(2,1)S(1)}, u32[]{:S(2)}) copy-start(bf16[48,4096]{1,0:T(8,128)(2,1)S(1)} %fusion.16) | copy-start | bytes 1179652
  196.4 110.9 %all-gather.7.cloned.1.call-start = ((), (), s32[]{:S(2)}) async-start(), calls=%async_computation.6 | async-start | bytes 1966080 | tf_op jit(solution)/shard_map/all_gather | solution.py:265
  197.2 191.2 %reduce-scatter.5.cloned.1.call-start = ((), (), s32[]{:S(2)}) async-start(), calls=%async_computation.8 | async-start | bytes 10485760 | tf_op jit(solution)/shard_map/reduce_scatter | solution.py:271
  307.1 128.4 %reduce-scatter.3.cloned.1.call-start = ((), (), s32[]{:S(2)}) async-start(), calls=%async_computation.7 | async-start | bytes 1966080 | tf_op jit(solution)/shard_map/reduce_scatter | solution.py:277
  307.4 2.8 copy-start.5
  388.4 7.7 %copy-start.12 = (f32[48,2]{0,1:T(2,128)S(1)}, f32[48,2]{0,1:T(2,128)}, u32[]{:S(2)}) copy-start(f32[48,2]{0,1:T(2,128)} %param.32) | copy-start | bytes 1156
  388.4 37.6 %all-to-all-start.2 = ((bf16[1,32,6,4096]{3,2,0,1:T(8,128)(2,1)}), bf16[1,32,6,4096]{3,2,0,1:T(8,128)(2,1)}, u32[]{:S(2)}, u32[]{:S(2)}) async-start(bf16[1,32,6,4096]{3,2,0,1:T(8,128)(2,1)} %bitcast.45), calls=%async_computation.4 | async-start | bytes 4194304 | tf_op jit(solution)/shard_map/all_to_all | solution.py:286
  431.7 5.0 %copy-start.9 = (f32[4096]{0:T(1024)S(1)}, f32[4096]{0:T(1024)}, u32[]{:S(2)}) copy-start(f32[4096]{0:T(1024)} %param.39) | copy-start | bytes 49156
  431.7 7.0 %copy-start.1 = (bf16[1,256,4096]{2,1,0:T(8,128)(2,1)S(1)}, bf16[1,256,4096]{2,1,0:T(8,128)(2,1)}, u32[]{:S(2)}) copy-start(bf16[1,256,4096]{2,1,0:T(8,128)(2,1)} %param.35) | copy-start | bytes 6291460
Sparse Core Ops, SparseCore 0:
  11.8 54.2 all-gather.4
  196.6 61.4 all-gather.8
  259.7 27.0 all-gather.6
  307.2 81.1 reduce-scatter.4
  390.7 25.3 reduce-scatter.2

commit v2 on v1

--- a/solution.py
+++ b/solution.py
@@ -17,17 +17,6 @@
 
 epsilon = 1e-06
 theta_base = 10000.0
-
-
-def cut_along(array, dim, count):
-    before, after = (array.shape[:dim], array.shape[dim + 1 :])
-    return jnp.moveaxis(array.reshape(*before, count, -1, *after), dim, 0)
-
-
-def sum_at_owner(array, axis, dim):
-    count = lax.axis_size(axis)
-    blocks = lax.all_to_all(cut_along(array, dim, count), axis, 0, 0, tiled=True)
-    return jnp.sum(blocks.astype(jnp.float32), axis=0)
 
 
 def rms_scale(values, gain_vector):
@@ -53,33 +42,6 @@
         ],
         axis=-1,
     )
-
-
-def expert_block(expert_in, gate_part, up_part, down_part):
-    hidden = (
-        jax.nn.silu(jnp.dot(expert_in, gate_part, preferred_element_type=jnp.float32))
-        * jnp.dot(expert_in, up_part, preferred_element_type=jnp.float32)
-    ).astype(jnp.bfloat16)
-    return jnp.dot(hidden, down_part, preferred_element_type=jnp.float32).astype(jnp.bfloat16)
-
-
-def dispatch_table(normed_rows, route_rows, experts, capacity):
-    row_count = normed_rows.shape[0]
-    flat_routes = route_rows.reshape(-1)
-    onehot = (flat_routes[:, None] == jnp.arange(experts, dtype=jnp.int32)[None, :]).astype(
-        jnp.int32
-    )
-    earlier = jnp.cumsum(onehot, axis=0) - onehot
-    target = flat_routes * capacity + jnp.sum(earlier * onehot, axis=1)
-    matches = (
-        target.reshape(row_count, -1)[None, :, :]
-        == jnp.arange(experts * capacity, dtype=jnp.int32)[:, None, None]
-    )
-    spread = jnp.any(matches, axis=2).astype(jnp.bfloat16)
-    slot_table = jnp.dot(spread, normed_rows, preferred_element_type=jnp.float32).astype(
-        jnp.bfloat16
-    )
-    return (slot_table.reshape(experts, capacity, normed_rows.shape[1]), target)
 
 
 BLK = 1024
@@ -205,6 +167,336 @@
         compiler_params=pltpu.CompilerParams(vmem_limit_bytes=48 * 1024 * 1024),
         name="attend",
     )(lat, qn, qr, wk, wv)
+
+
+MESH = pl.DeviceIdType.MESH
+SP, TP = 32, 4
+SLOTS = 24
+DIRECT_OUT = 1024
+DIRECT_BACK = 2048
+VM = pl.BlockSpec(memory_space=pltpu.VMEM)
+OFFSETS = ((0, 1), (1, 0), (0, 3), (3, 0), (0, 2), (2, 0), (1, 1), (3, 3), (1, 3), (3, 1), (1, 2), (2, 1), (3, 2), (2, 3), (2, 2))
+
+
+def remote(src, dst, send, recv, device):
+    return pltpu.make_async_remote_copy(
+        src_ref=src, dst_ref=dst, send_sem=send, recv_sem=recv, device_id=device, device_id_type=MESH
+    )
+
+
+def meet_tp(s, t):
+    bar = pltpu.get_barrier_semaphore()
+    for j in range(1, TP):
+        pl.semaphore_signal(bar, inc=1, device_id=(s, lax.rem(t + j, TP)), device_id_type=MESH)
+    return bar
+
+
+def meet_all(s, t):
+    bar = meet_tp(s, t)
+
+    def greet(k, carry):
+        pl.semaphore_signal(bar, inc=1, device_id=(lax.rem(s + k, SP), t), device_id_type=MESH)
+        return carry
+
+    lax.fori_loop(1, SP, greet, 0)
+    pl.semaphore_wait(bar, SP - 1 + TP - 1)
+
+
+def peers(s, k):
+    entry = lax.div(k + 1, 2) - 1
+    dc = lax.rem(k + 1, 2)
+    dz = jnp.int32(0)
+    dy = jnp.int32(0)
+    for i, (a, b) in enumerate(OFFSETS):
+        dz = jnp.where(entry == i, a, dz)
+        dy = jnp.where(entry == i, b, dy)
+    z, y, c = lax.div(s, 8), lax.rem(lax.div(s, 2), 4), lax.rem(s, 2)
+    to = lax.rem(z + dz, 4) * 8 + lax.rem(y + dy, 4) * 2 + lax.rem(c + dc, 2)
+    source = lax.rem(z - dz + 4, 4) * 8 + lax.rem(y - dy + 4, 4) * 2 + lax.rem(c + dc, 2)
+    return to, source
+
+
+def row_norm(values, gain):
+    return values * lax.rsqrt(jnp.mean(values * values, axis=-1, keepdims=True) + epsilon) * gain
+
+
+def mix_kernel(part, resid, gain, pre, side, mixed, group, sides, arrive, sems):
+    s, t = lax.axis_index("sp"), lax.axis_index("tp")
+    pl.semaphore_wait(meet_tp(s, t), TP - 1)
+
+    def to(j):
+        return (s, lax.rem(t + j, TP))
+
+    sums = [
+        remote(part.at[lax.rem(t + j, TP)], arrive.at[t], sems.at[0, j], sems.at[1, j], to(j)) for j in range(1, TP)
+    ]
+    extra = [remote(side, sides.at[t], sems.at[2, j], sems.at[3, j], to(j)) for j in range(1, TP)]
+    for copy in sums + extra:
+        copy.start()
+    sides[t] = side[...]
+    total = part[t].astype(jnp.float32)
+    for j in range(1, TP):
+        sums[j - 1].wait_recv()
+        total = total + arrive[lax.rem(t - j + TP, TP)].astype(jnp.float32)
+    mix = (resid[...].astype(jnp.float32) + row_norm(total, gain[...])).astype(jnp.bfloat16)
+    mixed[...] = mix
+    group[t] = row_norm(mix.astype(jnp.float32), pre[...]).astype(jnp.bfloat16)
+    gathers = [remote(group.at[t], group.at[t], sems.at[4, j], sems.at[5, j], to(j)) for j in range(1, TP)]
+    for copy in gathers:
+        copy.start()
+    for copy in extra + gathers:
+        copy.wait()
+    for copy in sums:
+        copy.wait_send()
+
+
+def mix_rows(part, resid, gain, pre, side):
+    rows, width = resid.shape
+    return pl.pallas_call(
+        mix_kernel,
+        out_shape=(
+            jax.ShapeDtypeStruct((rows, width), jnp.bfloat16),
+            jax.ShapeDtypeStruct((TP, rows, width), jnp.bfloat16),
+            jax.ShapeDtypeStruct((TP, rows, 128), jnp.float32),
+        ),
+        in_specs=[VM] * 5,
+        out_specs=(VM, VM, VM),
+        scratch_shapes=[pltpu.VMEM((TP, rows, width), jnp.bfloat16), pltpu.SemaphoreType.DMA((6, TP))],
+        compiler_params=pltpu.CompilerParams(collective_id=1, has_side_effects=True),
+        name="mix_rows",
+    )(part, resid, gain, pre, side)
+
+
+def finish_kernel(part, mixed, gain, out, arrive, sems):
+    s, t = lax.axis_index("sp"), lax.axis_index("tp")
+    pl.semaphore_wait(meet_tp(s, t), TP - 1)
+    sums = [
+        remote(part.at[lax.rem(t + j, TP)], arrive.at[t], sems.at[0, j], sems.at[1, j], (s, lax.rem(t + j, TP)))
+        for j in range(1, TP)
+    ]
+    for copy in sums:
+        copy.start()
+    total = part[t].astype(jnp.float32)
+    for j in range(1, TP):
+        sums[j - 1].wait_recv()
+        total = total + arrive[lax.rem(t - j + TP, TP)].astype(jnp.float32)
+    out[...] = (mixed[...].astype(jnp.float32) + row_norm(total, gain[...])).astype(jnp.bfloat16)
+    for copy in sums:
+        copy.wait_send()
+
+
+def finish(part, mixed, gain):
+    rows, width = mixed.shape
+    return pl.pallas_call(
+        finish_kernel,
+        out_shape=jax.ShapeDtypeStruct((rows, width), jnp.bfloat16),
+        in_specs=[VM] * 3,
+        out_specs=VM,
+        scratch_shapes=[pltpu.VMEM((TP, rows, width), jnp.bfloat16), pltpu.SemaphoreType.DMA((2, TP))],
+        compiler_params=pltpu.CompilerParams(collective_id=2, has_side_effects=True),
+        name="finish",
+    )(part, mixed, gain)
+
+
+def dispatch_kernel(table, out, qs, qr, ds, dr, fs, fr):
+    s, t = lax.axis_index("sp"), lax.axis_index("tp")
+    width = table.shape[2]
+    direct_cols = DIRECT_OUT
+    quarter_cols = (width - direct_cols) // TP
+    half = quarter_cols // 2
+    right, left, far = lax.rem(t + 1, TP), lax.rem(t + 3, TP), lax.rem(t + 2, TP)
+
+    def cols(owner, start, size):
+        return pl.ds(pl.multiple_of(direct_cols + owner * quarter_cols + start, 128), size)
+
+    mine = cols(t, 0, quarter_cols)
+    meet_all(s, t)
+
+    def quarter(k):
+        to, _ = peers(s, k)
+        return remote(table.at[to, :, mine], out.at[s, :, mine], qs.at[k], qr.at[k], (to, t))
+
+    def direct(k):
+        to, _ = peers(s, k)
+        at = pl.ds(0, direct_cols)
+        return remote(table.at[to, :, at], out.at[s, :, at], ds.at[k], dr.at[k], (to, t))
+
+    def relay(k, lane, owner, start, size, device):
+        _, source = peers(s, k)
+        block = out.at[source, :, cols(owner, start, size)]
+        return remote(block, block, fs.at[lane, k], fr.at[lane, k], (s, device))
+
+    def start_quarter(k, carry):
+        quarter(k).start()
+        return carry
+
+    def start_direct(k, carry):
+        direct(k).start()
+        return carry
+
+    lax.fori_loop(0, SP - 1, start_quarter, 0)
+    lax.fori_loop(0, SP - 1, start_direct, 0)
+    out[s] = table[s]
+
+    def first(k, carry):
+        quarter(k).wait_recv()
+        relay(k, 0, t, 0, quarter_cols, right).start()
+        relay(k, 1, t, 0, quarter_cols, left).start()
+        return carry
+
+    def second(k, carry):
+        relay(k, 0, left, 0, quarter_cols, left).wait_recv()
+        relay(k, 2, left, 0, half, right).start()
+        relay(k, 1, right, 0, quarter_cols, right).wait_recv()
+        relay(k, 3, right, half, half, left).start()
+        return carry
+
+    def last(k, carry):
+        relay(k, 2, far, 0, half, left).wait_recv()
+        relay(k, 3, far, half, half, right).wait_recv()
+        direct(k).wait_recv()
+        direct(k).wait_send()
+        quarter(k).wait_send()
+        relay(k, 0, t, 0, quarter_cols, right).wait_send()
+        relay(k, 1, t, 0, quarter_cols, left).wait_send()
+        relay(k, 2, left, 0, half, right).wait_send()
+        relay(k, 3, right, half, half, left).wait_send()
+        return carry
+
+    lax.fori_loop(0, SP - 1, first, 0)
+    lax.fori_loop(0, SP - 1, second, 0)
+    lax.fori_loop(0, SP - 1, last, 0)
+
+
+def dispatch(table):
+    dma = pltpu.SemaphoreType.DMA
+    return pl.pallas_call(
+        dispatch_kernel,
+        out_shape=jax.ShapeDtypeStruct(table.shape, table.dtype),
+        in_specs=[VM],
+        out_specs=VM,
+        scratch_shapes=[dma((SP,)), dma((SP,)), dma((SP,)), dma((SP,)), dma((TP, SP)), dma((TP, SP))],
+        compiler_params=pltpu.CompilerParams(
+            collective_id=3, has_side_effects=True, vmem_limit_bytes=32 * 1024 * 1024
+        ),
+        name="dispatch",
+    )(table)
+
+
+def bring_kernel(rows, out, arrive, summed, qs, qr, ds, dr, xs, xr):
+    s, t = lax.axis_index("sp"), lax.axis_index("tp")
+    direct_cols = DIRECT_BACK
+    quarter_cols = (rows.shape[2] - direct_cols) // TP
+
+    def cols(owner):
+        return pl.ds(pl.multiple_of(direct_cols + owner * quarter_cols, 128), quarter_cols)
+
+    lead, tail = pl.ds(0, direct_cols), pl.ds(direct_cols, quarter_cols)
+    meet_all(s, t)
+
+    def block(k):
+        return peers(s, k)[0]
+
+    def direct(k):
+        to = block(k)
+        return remote(rows.at[to, :, lead], out.at[s, :, lead], ds.at[k], dr.at[k], (to, t))
+
+    def quarter(k):
+        to = block(k)
+        return remote(summed.at[to], out.at[s, :, tail], qs.at[k], qr.at[k], (to, t))
+
+    def cross(b, j):
+        owner = lax.rem(t + j, TP)
+        return remote(rows.at[b, :, cols(owner)], arrive.at[j, b], xs.at[j, b], xr.at[j, b], (s, owner))
+
+    def launch(k, carry):
+        for j in (2, 1, 3):
+            cross(block(k), j).start()
+        direct(k).start()
+        return carry
+
+    def add_up(b):
+        total = rows[b, :, cols(t)].astype(jnp.float32)
+        for j in range(1, TP):
+            cross(b, j).wait_recv()
+            total = total + arrive[j, b].astype(jnp.float32)
+        return total.astype(jnp.bfloat16)
+
+    def forward(k, carry):
+        b = block(k)
+        summed[b] = add_up(b)
+        quarter(k).start()
+        return carry
+
+    def last(k, carry):
+        direct(k).wait()
+        quarter(k).wait()
+        for j in range(1, TP):
+            cross(block(k), j).wait_send()
+        return carry
+
+    lax.fori_loop(0, SP - 1, launch, 0)
+    for j in (2, 1, 3):
+        cross(s, j).start()
+    out[s, :, 0:direct_cols] = rows[s, :, 0:direct_cols]
+    lax.fori_loop(0, SP - 1, forward, 0)
+    out[s, :, direct_cols:] = add_up(s)
+    for j in range(1, TP):
+        cross(s, j).wait_send()
+    lax.fori_loop(0, SP - 1, last, 0)
+
+
+def bring(rows):
+    quarter_cols = (rows.shape[2] - DIRECT_BACK) // TP
+    dma = pltpu.SemaphoreType.DMA
+    return pl.pallas_call(
+        bring_kernel,
+        out_shape=jax.ShapeDtypeStruct((SP, SLOTS, DIRECT_BACK + quarter_cols), rows.dtype),
+        in_specs=[VM],
+        out_specs=VM,
+        scratch_shapes=[
+            pltpu.VMEM((TP, SP, SLOTS, quarter_cols), jnp.bfloat16),
+            pltpu.VMEM((SP, SLOTS, quarter_cols), jnp.bfloat16),
+            dma((SP,)),
+            dma((SP,)),
+            dma((SP,)),
+            dma((SP,)),
+            dma((TP, SP)),
+            dma((TP, SP)),
+        ],
+        compiler_params=pltpu.CompilerParams(
+            collective_id=4, has_side_effects=True, vmem_limit_bytes=32 * 1024 * 1024
+        ),
+        name="bring",
+    )(rows)
+
+
+def expert_kernel(x, gate, up, down, out):
+    step = 192
+
+    def chunk(i, carry):
+        at = pl.ds(pl.multiple_of(i * step, step), step)
+        rows = x[at, :]
+        g = jnp.dot(rows, gate[...], preferred_element_type=jnp.float32)
+        u = jnp.dot(rows, up[...], preferred_element_type=jnp.float32)
+        hidden = (g / (1.0 + jnp.exp(-g)) * u).astype(jnp.bfloat16)
+        for n in range(4):
+            cs = pl.ds(n * 1024, 1024)
+            out[at, cs] = jnp.dot(hidden, down[:, cs], preferred_element_type=jnp.float32).astype(jnp.bfloat16)
+        return carry
+
+    lax.fori_loop(0, x.shape[0] // step, chunk, 0)
+
+
+def expert_rows(x, gate, up, down, name):
+    return pl.pallas_call(
+        expert_kernel,
+        out_shape=jax.ShapeDtypeStruct(x.shape, jnp.bfloat16),
+        in_specs=[VM] * 4,
+        out_specs=VM,
+        compiler_params=pltpu.CompilerParams(vmem_limit_bytes=32 * 1024 * 1024),
+        name=name,
+    )(x, gate, up, down)
 
 
 def on_device(
@@ -248,49 +540,50 @@
         key_up,
         value_up,
     )
-    projected = sum_at_owner(
-        jnp.dot(attention, out_proj, preferred_element_type=jnp.float32).astype(jnp.bfloat16),
-        "tp",
-        0,
-    )
-    mixed = (resid.astype(jnp.float32) + rms_scale(projected, attn_gain)).astype(jnp.bfloat16)
-    normed = rms_scale(mixed.astype(jnp.float32), pre_gain).astype(jnp.bfloat16)
     rows_here = resid.shape[0]
-    tp_count = lax.axis_size("tp")
-    experts = lax.axis_size("sp")
-    capacity = max(2, 2 * rows_here * TOP_K // experts)
-    own_table, target = dispatch_table(normed, routes, experts, capacity)
-    arrived = lax.all_to_all(own_table, "sp", split_axis=0, concat_axis=0, tiled=True)
-    column = lax.all_gather(arrived[None], "tp", axis=0, tiled=True)
-    group_normed = lax.all_gather(normed, "tp", axis=0, tiled=True)
-    expert_out = expert_block(
-        column.reshape(-1, MODEL_DIM), expert_gate[0], expert_up[0], expert_down[0]
-    )
-    shared_part = expert_block(group_normed, shared_gate, shared_up, shared_down)
-    routed_sum, shared_sum = (
-        lax.psum_scatter(
-            expert_out.reshape(column.shape).astype(jnp.float32).astype(jnp.bfloat16),
-            "tp",
-            scatter_dimension=0,
-            tiled=True,
-        ).astype(jnp.float32),
-        lax.psum_scatter(
-            shared_part.reshape(tp_count, rows_here, MODEL_DIM)
-            .astype(jnp.float32)
-            .astype(jnp.bfloat16),
-            "tp",
-            scatter_dimension=0,
-            tiled=True,
-        ).astype(jnp.float32),
-    )
-    expert_rows = lax.all_to_all(
-        routed_sum.astype(jnp.bfloat16), "sp", split_axis=1, concat_axis=1, tiled=True
-    ).reshape(-1, MODEL_DIM)
-    shared_out = shared_sum.reshape(rows_here, MODEL_DIM)
-    picked = expert_rows[target].astype(jnp.float32).reshape(rows_here, TOP_K, MODEL_DIM)
-    routed = jnp.sum(picked * route_weights[..., None], axis=1)
-    moe = shared_out + routed
-    return (mixed.astype(jnp.float32) + rms_scale(moe, moe_gain)).astype(jnp.bfloat16)
+    tp_index = lax.axis_index("tp")
+    capacity = SLOTS // TP
+    flat_routes = routes.reshape(-1)
+    onehot = (flat_routes[:, None] == jnp.arange(SP, dtype=jnp.int32)[None, :]).astype(jnp.int32)
+    earlier = jnp.cumsum(onehot, axis=0) - onehot
+    target = flat_routes * SLOTS + tp_index * capacity + jnp.sum(earlier * onehot, axis=1)
+    side = jnp.concatenate(
+        [
+            target.reshape(rows_here, TOP_K).astype(jnp.float32),
+            route_weights,
+            jnp.zeros((rows_here, 128 - 2 * TOP_K), jnp.float32),
+        ],
+        axis=1,
+    )
+    part = jnp.dot(attention, out_proj, preferred_element_type=jnp.float32).astype(jnp.bfloat16)
+    mixed, group, sides = mix_rows(
+        part.reshape(TP, rows_here, MODEL_DIM), resid, attn_gain[None], pre_gain[None], side
+    )
+    group = group.reshape(TP * rows_here, MODEL_DIM)
+    sides = sides.reshape(TP * rows_here, 128)
+    slots = jnp.arange(SP * SLOTS, dtype=jnp.int32).astype(jnp.float32)
+    spread = ((sides[:, 0][None] == slots[:, None]) | (sides[:, 1][None] == slots[:, None])).astype(jnp.bfloat16)
+    table = jnp.dot(spread, group, preferred_element_type=jnp.float32).astype(jnp.bfloat16)
+    arrived = dispatch(table.reshape(SP, SLOTS, MODEL_DIM))
+    expert_out = expert_rows(
+        arrived.reshape(SP * SLOTS, MODEL_DIM), expert_gate[0], expert_up[0], expert_down[0], "expert"
+    )
+    shared_part = expert_rows(group, shared_gate, shared_up, shared_down, "shared")
+    back = bring(expert_out.reshape(SP, SLOTS, MODEL_DIM)).reshape(SP * SLOTS, -1)
+    picks = jnp.where(sides[:, 0:1] == slots[None], sides[:, 2:3], 0.0) + jnp.where(
+        sides[:, 1:2] == slots[None], sides[:, 3:4], 0.0
+    )
+    high = picks.astype(jnp.bfloat16)
+    low = (picks - high.astype(jnp.float32)).astype(jnp.bfloat16)
+    routed = jnp.dot(high, back, preferred_element_type=jnp.float32) + jnp.dot(
+        low, back, preferred_element_type=jnp.float32
+    )
+    lead = shared_part[:, :DIRECT_BACK].astype(jnp.float32) + routed[:, :DIRECT_BACK]
+    tail = shared_part[:, DIRECT_BACK:].astype(jnp.float32) + jnp.concatenate(
+        [jnp.where(tp_index == c, routed[:, DIRECT_BACK:], 0.0) for c in range(TP)], axis=1
+    )
+    total = jnp.concatenate([lead.astype(jnp.bfloat16), tail.astype(jnp.bfloat16)], axis=1)
+    return finish(total.reshape(TP, rows_here, MODEL_DIM), mixed, moe_gain[None])
 
 
 def solution(mesh):

time: 447 us -> 328 us (0.73)
  Pallas kernels: 24.1 us -> 239 us
  waiting for transfers between devices: 235 us -> 52.1 us
  blocking collectives: 65.3 us -> 0 us
  local copies, waits for them, and re-layouts: 49.2 us -> 8.33 us
  matrix products: 31.7 us -> 8.29 us
  starting transfers between devices: 12.6 us -> 0.01 us
  other arithmetic: 14 us -> 5.91 us
    pallas_call x0 -> x6, Pallas kernels: none -> 215 us  [the longest x1 79.7 us: dispatch(): pl.pallas_call(dispatch_kernel, out_shape=jax.ShapeDtypeStruct(table.shap...]
    reduce_scatter x2 -> x0, waiting for transfers between devices: 73 us -> none  [the longest x1 73 us: on_device(): lax.psum_scatter(expert_out.reshape(column.shape).astype(jnp.float32).ast...]
    all_to_all x1 -> x0, blocking collectives: 65.3 us -> none  [on_device(): lax.all_to_all(own_table, 'sp', split_axis=0, concat_axis=0, tiled=True)]
    all_gather x2 -> x0, waiting for transfers between devices: 60.7 us -> none  [the longest x1 60.7 us: on_device(): column = lax.all_gather(arrived[None], 'tp', axis=0, tiled=True)]
    all_to_all x2 -> x0, waiting for transfers between devices: 50.2 us -> none  [the longest x1 29.8 us: on_device(): lax.all_to_all(routed_sum.astype(jnp.bfloat16), 'sp', split_axis=1, conca...]
    reshape x4 -> x0, local copies, waits for them, and re-layouts: 26.4 us -> none  [the longest x1 10.3 us: on_device(): column.reshape(-1, MODEL_DIM)]
    dot_general x5 -> x3, matrix products: 28.7 us -> 5.32 us  [the longest x1 3.26 us: on_device(): jnp.dot(spread, group, preferred_element_type=jnp.float32)]
    all_to_all x2 -> x0, starting transfers between devices: 12 us -> none  [the longest x1 7.53 us: on_device(): lax.all_to_all(routed_sum.astype(jnp.bfloat16), 'sp', split_axis=1, conca...]
  transfers between devices with their start and end apart: 7 -> 1, of which waited for: 5 -> 1; matrix products, arithmetic and copies ran while one was open for 16% -> 1% of each run, Pallas kernels for 0% -> 0%
where the time goes in v2:
time: 328 us; the launch traced here: 327 us
  Pallas kernels  239 us (73%)
  waiting for transfers between devices  52.1 us (16%)
  between operations  13.7 us (4%)
  local copies, waits for them, and re-layouts  8.33 us (3%)
  matrix products  8.29 us (3%)
  other arithmetic  5.91 us (2%)
    pallas_call x1, Pallas kernels, dispatch(): pl.pallas_call(dispatch_kernel, out_shape=jax.ShapeDtypeStruct(table.shap...  79.7 us
    pallas_call x1, Pallas kernels, bring(): pl.pallas_call(bring_kernel, out_shape=jax.ShapeDtypeStruct((SP, SLOTS, D...  57.3 us
    all_gather x1, waiting for transfers between devices, on_device(): lax.all_gather(jnp.concatenate([latent_normed] + [key_rot] * 4, axis=1),...  52.1 us
    pallas_call x1, Pallas kernels, mix_rows(): pl.pallas_call(mix_kernel, out_shape=(jax.ShapeDtypeStruct((rows, width),...  45.5 us
    pallas_call x1, Pallas kernels, finish(): pl.pallas_call(finish_kernel, out_shape=jax.ShapeDtypeStruct((rows, width...  24.4 us
    pallas_call x1, Pallas kernels, attend(): pl.pallas_call(functools.partial(attend_kernel, index_fn), out_shape=jax....  24.3 us
    pallas_call x2, Pallas kernels, expert_rows(): pl.pallas_call(expert_kernel, out_shape=jax.ShapeDtypeStruct(x.shape, jnp...  7.58 us
  transfers between devices with their start and end apart: 1, of which 1 were waited for; matrix products, arithmetic and copies ran while one was open for 1% of the time, Pallas kernels for 0%

profile of v2, /device:TPU:0, one launch (start us, length us, event | category | flops | bytes accessed | tf_op | source)
XLA Modules:
  0.0 327.3 jit_solution(11965735980042986486)
XLA Ops:
  6.6 1.1 fusion.6
  7.7 0.8 copy.41
  8.6 1.0 fusion.8
  9.6 0.5 multiply_cosine_fusion
  10.1 0.9 concatenate.19
  11.0 0.0 all-gather.2.cloned.1.call-update
  11.0 0.1 copy.47
  11.1 0.1 copy.48
  11.2 0.1 copy.49
  11.3 0.1 eq.83
  11.4 0.1 fusion.21
  11.5 0.1 reduce_window_sum.11
  11.6 0.2 select_reduce_fusion
  11.8 0.1 reduce_sum.22
  11.9 0.1 copy.44
  12.0 0.1 copy.45
  12.1 0.1 copy.43
  12.3 0.1 subtract_convert_fusion.2
  12.4 0.1 copy.46.qr_ref
  12.6 0.1 pad.8.clone
  12.6 0.7 maximum_maximum_fusion.side
  13.3 52.1 %all-gather.2.cloned.1.call-done.lat_ref = bf16[6144,640]{1,0:T(8,128)(2,1)} async-done(((bf16[192,640]{1,0:T(8,128)(2,1)}), bf16[6144,640]{1,0:T(8,128)(2,1)}) %all-gather.2.cloned.1.call-update) | async-done | bytes 7864336 | tf_op jit(solution)/shard_map/all_gather | solution.py:529
  65.4 24.3 %attend.1 = bf16[192,1024]{1,0:T(8,128)(2,1)S(1)} custom-call(bf16[6144,640]{1,0:T(8,128)(2,1)} %all-gather.2.cloned.1.call-done.lat_ref, bf16[192,1024]{1,0:T(8,128)(2,1)S(1)} %copy-done.9, bf16[192,512]{1,0:T(8,128)(2,1)S(1)} %copy.46.qr_ref, bf16[512,1024]{1,0:T(8,128)(2,1)S(1)} %copy-done.7, bf16[512,1024]{1,0:T(8,128)(2,1)S(1)} %copy-done.8), custom_call_target="tpu_custom_call" | custom-call | tf_op jit(solution)/shard_map/attend/pallas_call | solution.py:153
  89.7 3.0 convolution_convert_fusion.1
  92.7 45.5 %mix_rows.1 = (bf16[48,4096]{1,0:T(8,128)(2,1)}, bf16[4,48,4096]{2,1,0:T(8,128)(2,1)}, f32[4,48,128]{2,1,0:T(8,128)}) custom-call(bf16[4,48,4096]{2,1,0:T(8,128)(2,1)} %bitcast.38, bf16[48,4096]{1,0:T(8,128)(2,1)} %resid.1, f32[1,4096]{1,0:T(1,128)} %bitcast.47, f32[1,4096]{1,0:T(1,128)} %bitcast.48, f32[48,128]{1,0:T(8,128)} %maximum_maximum_fusion.side), custom_call_target="tpu_custom_call" | custom-call | tf_op jit(solution)/shard_map/mix_rows/pallas_call | solution.py:255
  138.2 1.2 fusion.24
  139.4 0.1 copy.55
  139.5 0.1 copy.56
  139.6 0.1 copy.54
  139.7 0.1 copy.57
  139.8 3.3 convolution_convert_fusion
  143.1 0.0 copy-start.3
  143.1 79.7 %dispatch.1 = bf16[32,24,4096]{2,1,0:T(8,128)(2,1)S(1)} custom-call(bf16[32,24,4096]{2,1,0:T(8,128)(2,1)S(1)} %bitcast.28), custom_call_target="tpu_custom_call" | custom-call | tf_op jit(solution)/shard_map/dispatch/pallas_call | solution.py:373
  222.8 6.1 %expert.1 = bf16[768,4096]{1,0:T(8,128)(2,1)S(1)} custom-call(bf16[768,4096]{1,0:T(8,128)(2,1)S(1)} %bitcast.29, bf16[4096,256]{1,0:T(8,128)(2,1)S(1)} %bitcast.33, bf16[4096,256]{1,0:T(8,128)(2,1)S(1)} %bitcast.34, bf16[256,4096]{1,0:T(8,128)(2,1)S(1)} %bitcast.35), custom_call_target="tpu_custom_call" | custom-call | tf_op jit(solution)/shard_map/expert/pallas_call | solution.py:492
  228.9 57.3 %bring.1 = bf16[32,24,2560]{2,1,0:T(8,128)(2,1)S(1)} custom-call(bf16[32,24,4096]{2,1,0:T(8,128)(2,1)S(1)} %bitcast.30), custom_call_target="tpu_custom_call" | custom-call | tf_op jit(solution)/shard_map/bring/pallas_call | solution.py:452
  286.3 1.0 fusion.19
  287.3 0.0 copy-start.5
  287.3 1.0 convolution_add_fusion
  288.4 0.3 copy-done
  288.7 0.7 copy-done.4
  289.4 0.6 copy-done.5
  290.0 0.6 copy-done.6
  290.6 1.5 shared.1
  292.2 0.2 slice_select_fusion.3
  292.4 0.5 fusion
  292.9 1.3 pad_maximum_fusion
  294.2 24.4 %finish.1 = bf16[48,4096]{1,0:T(8,128)(2,1)} custom-call(bf16[4,48,4096]{2,1,0:T(8,128)(2,1)} %bitcast.36, bf16[48,4096]{1,0:T(8,128)(2,1)} %get-tuple-element.10.mixed, f32[1,4096]{1,0:T(1,128)} %bitcast.49), custom_call_target="tpu_custom_call" | custom-call | tf_op jit(solution)/shard_map/finish/pallas_call | solution.py:290
  318.6 1.8 copy.59
  (33 shorter events, 0.2 us)
Async XLA Ops:
  6.5 4.5 %copy-start.11 = (s32[48,2]{0,1:T(2,128)S(1)}, s32[48,2]{0,1:T(2,128)}, u32[]{:S(2)}) copy-start(s32[48,2]{0,1:T(2,128)} %param.31) | copy-start | bytes 1156
  6.5 4.7 %copy-start.12 = (f32[48,2]{0,1:T(2,128)S(1)}, f32[48,2]{0,1:T(2,128)}, u32[]{:S(2)}) copy-start(f32[48,2]{0,1:T(2,128)} %param.32) | copy-start | bytes 1156
  6.5 5.5 %copy-start.10 = (bf16[192,512]{1,0:T(8,128)(2,1)S(1)}, bf16[192,512]{1,0:T(8,128)(2,1)}, u32[]{:S(2)}) copy-start(bf16[192,512]{1,0:T(8,128)(2,1)} %param.21) | copy-start | bytes 589828
  6.5 58.9 %all-gather.2.cloned.1.call-start = ((), (), s32[]{:S(2)}) async-start(), calls=%async_computation | async-start | bytes 8110080 | tf_op jit(solution)/shard_map/all_gather | solution.py:529
  10.9 54.5 %copy-start.7 = (bf16[512,1024]{1,0:T(8,128)(2,1)S(1)}, bf16[512,1024]{1,0:T(8,128)(2,1)}, u32[]{:S(2)}) copy-start(bf16[512,1024]{1,0:T(8,128)(2,1)} %wk_ref.1) | copy-start | bytes 3145732
  11.0 54.5 %copy-start.8 = (bf16[512,1024]{1,0:T(8,128)(2,1)S(1)}, bf16[512,1024]{1,0:T(8,128)(2,1)}, u32[]{:S(2)}) copy-start(bf16[512,1024]{1,0:T(8,128)(2,1)} %wv_ref.1) | copy-start | bytes 3145732
  11.0 54.5 %copy-start.9 = (bf16[192,1024]{1,0:T(8,128)(2,1)S(1)}, bf16[192,1024]{1,0:T(8,128)(2,1)}, u32[]{:S(2)}) copy-start(bf16[192,1024]{1,0:T(8,128)(2,1)} %qn_ref.1) | copy-start | bytes 1179652
  65.4 24.3 %copy-start.13 = (bf16[1024,4096]{1,0:T(8,128)(2,1)S(1)}, bf16[1024,4096]{1,0:T(8,128)(2,1)}, u32[]{:S(2)}) copy-start(bf16[1024,4096]{1,0:T(8,128)(2,1)} %param.27) | copy-start | bytes 25165828
  143.0 79.8 %copy-start.1 = (bf16[1,4096,256]{2,1,0:T(8,128)(2,1)S(1)}, bf16[1,4096,256]{2,1,0:T(8,128)(2,1)}, u32[]{:S(2)}) copy-start(bf16[1,4096,256]{2,1,0:T(8,128)(2,1)} %param.33) | copy-start | bytes 6291460
  143.0 79.8 %copy-start.2 = (bf16[1,4096,256]{2,1,0:T(8,128)(2,1)S(1)}, bf16[1,4096,256]{2,1,0:T(8,128)(2,1)}, u32[]{:S(2)}) copy-start(bf16[1,4096,256]{2,1,0:T(8,128)(2,1)} %param.34) | copy-start | bytes 6291460
  143.1 79.8 %copy-start.3 = (bf16[1,256,4096]{2,1,0:T(8,128)(2,1)S(1)}, bf16[1,256,4096]{2,1,0:T(8,128)(2,1)}, u32[]{:S(2)}) copy-start(bf16[1,256,4096]{2,1,0:T(8,128)(2,1)} %param.35) | copy-start | bytes 6291460
  287.3 1.4 copy-start
  287.3 2.1 copy-start.4
  287.3 2.7 copy-start.5
  287.3 3.3 %copy-start.6 = (bf16[256,4096]{1,0:T(8,128)(2,1)S(1)}, bf16[256,4096]{1,0:T(8,128)(2,1)}, u32[]{:S(2)}) copy-start(bf16[256,4096]{1,0:T(8,128)(2,1)} %down.1) | copy-start | bytes 6291460
Sparse Core Ops, SparseCore 0:
  11.1 54.2 all-gather.1

commit v3 on v2

--- a/solution.py
+++ b/solution.py
@@ -469,6 +469,124 @@
         ),
         name="bring",
     )(rows)
+
+
+def gather_kernel(block, out, su, ru, sv, rv, sr, rr, sd, rd):
+    s, t = lax.axis_index("sp"), lax.axis_index("tp")
+    z, y, c = lax.div(s, 8), lax.rem(lax.div(s, 2), 4), lax.rem(s, 2)
+    rows = block.shape[0]
+    half = rows // 2
+    part = half // 2
+    other = 1 - c
+
+    def index(h, u, v, core):
+        zz, yy = (v, u) if h == 0 else (u, v)
+        return zz * 8 + yy * 2 + core
+
+    def here(h):
+        return (y, z) if h == 0 else (z, y)
+
+    def back(x, j):
+        return lax.rem(x - j + 4, 4)
+
+    def piece(h, u, v, core, start, size):
+        return out.at[index(h, u, v, core), pl.ds(h * half + start, size), :]
+
+    bar = pltpu.get_barrier_semaphore()
+    for j in range(1, 4):
+        for device in (index(0, lax.rem(y + j, 4), z, c), index(0, y, lax.rem(z + j, 4), c)):
+            pl.semaphore_signal(bar, inc=1, device_id=(device, t), device_id_type=MESH)
+    pl.semaphore_signal(bar, inc=1, device_id=(index(0, y, z, other), t), device_id_type=MESH)
+    pl.semaphore_wait(bar, 7)
+
+    pending = []
+
+    def send(src, dst, ss, rs, device):
+        copy = remote(src, dst, ss, rs, (device, t))
+        copy.start()
+        pending.append(copy)
+
+    def wait(dst, ss, rs):
+        remote(dst, dst, ss, rs, (index(0, y, z, other), t)).wait_recv()
+
+    def own(h):
+        return block.at[pl.ds(h * half, half), :]
+
+    def share(h, a, b, src=None):
+        u, v = here(h)
+        dst = piece(h, back(u, a), back(v, b), c, 0, half)
+        send(dst if src is None else src, dst, sd.at[h, a, b], rd.at[h, a, b], index(0, y, z, other))
+
+    def along(h, a, src=None):
+        u, v = here(h)
+        dst = piece(h, back(u, a), v, c, 0, half)
+        for lane, j in ((0, 1), (1, 3)):
+            device = index(h, u, lax.rem(v + j, 4), c)
+            send(dst if src is None else src, dst, sv.at[h, a, lane], rv.at[h, a, lane], device)
+
+    for j in (1, 3, 2):
+        for h in range(2):
+            u, v = here(h)
+            send(own(h), piece(h, u, v, c, 0, half), su.at[h, j], ru.at[h, j], index(h, lax.rem(u + j, 4), v, c))
+    for h in range(2):
+        along(h, 0, own(h))
+        share(h, 0, 0, own(h))
+    out[s] = block[...]
+    for a in (1, 3, 2):
+        for h in range(2):
+            u, v = here(h)
+            wait(piece(h, back(u, a), v, c, 0, half), su.at[h, a], ru.at[h, a])
+            along(h, a)
+            share(h, a, 0)
+    for a in (0, 1, 3, 2):
+        for h in range(2):
+            u, v = here(h)
+            for lane, j in ((0, 1), (1, 3)):
+                ua, vb = back(u, a), back(v, j)
+                wait(piece(h, ua, vb, c, 0, half), sv.at[h, a, lane], rv.at[h, a, lane])
+                block_part = piece(h, ua, vb, c, lane * part, part)
+                device = index(h, u, lax.rem(v + j, 4), c)
+                send(block_part, block_part, sr.at[h, a, lane], rr.at[h, a, lane], device)
+                share(h, a, j)
+    for a in (0, 1, 3, 2):
+        for h in range(2):
+            u, v = here(h)
+            for lane in range(2):
+                dst = piece(h, back(u, a), back(v, 2), c, lane * part, part)
+                wait(dst, sr.at[h, a, lane], rr.at[h, a, lane])
+            share(h, a, 2)
+    for h in range(2):
+        u, v = here(h)
+        for a in range(4):
+            for b in range(4):
+                wait(piece(h, back(u, a), back(v, b), other, 0, half), sd.at[h, a, b], rd.at[h, a, b])
+    for copy in pending:
+        copy.wait_send()
+
+
+def gather_latents(block):
+    rows, width = block.shape
+    dma = pltpu.SemaphoreType.DMA
+    return pl.pallas_call(
+        gather_kernel,
+        out_shape=jax.ShapeDtypeStruct((SP, rows, width), block.dtype),
+        in_specs=[VM],
+        out_specs=VM,
+        scratch_shapes=[
+            dma((2, 4)),
+            dma((2, 4)),
+            dma((2, 4, 2)),
+            dma((2, 4, 2)),
+            dma((2, 4, 2)),
+            dma((2, 4, 2)),
+            dma((2, 4, 4)),
+            dma((2, 4, 4)),
+        ],
+        compiler_params=pltpu.CompilerParams(
+            collective_id=5, has_side_effects=True, vmem_limit_bytes=32 * 1024 * 1024
+        ),
+        name="gather_latents",
+    )(block)
 
 
 def expert_kernel(x, gate, up, down, out):
@@ -526,9 +644,8 @@
     query_pos = lax.axis_index("sp") * local_rows + jnp.arange(local_rows, dtype=jnp.int32)
     key_rot = rotate(key_rope.astype(jnp.float32), query_pos).astype(jnp.bfloat16)
     latent_normed = rms_scale(latent.astype(jnp.float32), latent_gain).astype(jnp.bfloat16)
-    latent_all = lax.all_gather(
-        jnp.concatenate([latent_normed] + [key_rot] * 4, axis=1), "sp", axis=0, tiled=True
-    )
+    latent_all = gather_latents(jnp.concatenate([latent_normed] + [key_rot] * 4, axis=1))
+    latent_all = latent_all.reshape(-1, latent_all.shape[2])
     query_rot = rotate(
         query_rope.astype(jnp.float32).reshape(local_rows, heads_here, ROPE_DIM), query_pos[:, None]
     ).astype(jnp.bfloat16)

time: 328 us -> 305 us (0.930)
  waiting for transfers between devices: 52.1 us -> 0 us
  Pallas kernels: 239 us -> 272 us
  between operations: 13.7 us -> 0.33 us
  local copies, waits for them, and re-layouts: 8.33 us -> 14.4 us
    all_gather x1 -> x0, waiting for transfers between devices: 52.1 us -> none  [on_device(): lax.all_gather(jnp.concatenate([latent_normed] + [key_rot] * 4, axis=1),...]
    pallas_call x0 -> x1, Pallas kernels: none -> 31.4 us  [gather_latents(): pl.pallas_call(gather_kernel, out_shape=jax.ShapeDtypeStruct((SP, rows, w...]
    unnamed x37 -> x35, local copies, waits for them, and re-layouts: 5.56 us -> 12.3 us
    dot_general x1, matrix products: 2.97 us -> 6.34 us  [on_device(): jnp.dot(attention, out_proj, preferred_element_type=jnp.float32)]
  transfers between devices with their start and end apart: 1 -> 0, of which waited for: 1 -> 0; matrix products, arithmetic and copies ran while one was open for 1% -> 0% of each run, Pallas kernels for 0% -> 0%
where the time goes in v3:
time: 305 us; the launch traced here: 304 us
  Pallas kernels  272 us (89%)
  local copies, waits for them, and re-layouts  14.4 us (5%)
  matrix products  10.2 us (3%)
  other arithmetic  6.58 us (2%)
    pallas_call x1, Pallas kernels, dispatch(): pl.pallas_call(dispatch_kernel, out_shape=jax.ShapeDtypeStruct(table.shap...  80 us
    pallas_call x1, Pallas kernels, bring(): pl.pallas_call(bring_kernel, out_shape=jax.ShapeDtypeStruct((SP, SLOTS, D...  59.3 us
    pallas_call x1, Pallas kernels, mix_rows(): pl.pallas_call(mix_kernel, out_shape=(jax.ShapeDtypeStruct((rows, width),...  45.8 us
    pallas_call x1, Pallas kernels, gather_latents(): pl.pallas_call(gather_kernel, out_shape=jax.ShapeDtypeStruct((SP, rows, w...  31.4 us
    pallas_call x1, Pallas kernels, attend(): pl.pallas_call(functools.partial(attend_kernel, index_fn), out_shape=jax....  24.1 us
    pallas_call x1, Pallas kernels, finish(): pl.pallas_call(finish_kernel, out_shape=jax.ShapeDtypeStruct((rows, width...  24 us
    unnamed x35, local copies, waits for them, and re-layouts  12.3 us
    pallas_call x2, Pallas kernels, expert_rows(): pl.pallas_call(expert_kernel, out_shape=jax.ShapeDtypeStruct(x.shape, jnp...  7.76 us

profile of v3, /device:TPU:0, one launch (start us, length us, event | category | flops | bytes accessed | tf_op | source)
XLA Modules:
  0.0 303.9 jit_solution(9169493162584007519)
XLA Ops:
  0.0 0.7 multiply_add_fusion
  0.7 0.1 pad.8.clone
  0.8 1.1 fusion.6
  1.9 0.1 copy.48
  2.0 0.8 copy.49
  2.8 0.8 copy.47
  3.5 0.1 eq.83
  3.6 0.1 fusion.21
  3.7 0.1 reduce_window_sum.11
  3.9 0.2 select_reduce_fusion
  4.0 0.1 reduce_sum.22
  4.2 0.7 maximum_maximum_fusion.side
  4.9 0.8 copy.41
  5.7 0.5 multiply_cosine_fusion
  6.2 0.1 copy.44
  6.2 0.1 copy.45
  6.3 1.1 fusion.8
  7.4 0.2 concatenate.19.block
  7.6 0.1 copy.43
  7.8 0.1 subtract_convert_fusion.2
  7.9 0.1 copy.46.qr_ref
  8.1 0.0 copy-start.10
  8.1 0.0 copy-start.11
  8.1 31.4 %gather_latents.1 = bf16[32,192,640]{2,1,0:T(8,128)(2,1)S(1)} custom-call(bf16[192,640]{1,0:T(8,128)(2,1)S(1)} %concatenate.19.block), custom_call_target="tpu_custom_call" | custom-call | tf_op jit(solution)/shard_map/gather_latents/pallas_call | solution.py:570
  39.5 3.1 %copy-done = bf16[32,192,640]{2,1,0:T(8,128)(2,1)} copy-done((bf16[32,192,640]{2,1,0:T(8,128)(2,1)}, bf16[32,192,640]{2,1,0:T(8,128)(2,1)S(1)}, u32[]{:S(2)}) %copy-start) | copy-done | bytes 7864344
  42.5 24.1 %attend.1 = bf16[192,1024]{1,0:T(8,128)(2,1)S(1)} custom-call(bf16[6144,640]{1,0:T(8,128)(2,1)} %bitcast.30, bf16[192,1024]{1,0:T(8,128)(2,1)S(1)} %copy-done.11, bf16[192,512]{1,0:T(8,128)(2,1)S(1)} %copy.46.qr_ref, bf16[512,1024]{1,0:T(8,128)(2,1)S(1)} %copy-done.9, bf16[512,1024]{1,0:T(8,128)(2,1)S(1)} %copy-done.10), custom_call_target="tpu_custom_call" | custom-call | tf_op jit(solution)/shard_map/attend/pallas_call | solution.py:153
  66.6 6.3 %convolution_convert_fusion.1 = bf16[192,4096]{1,0:T(8,128)(2,1)} fusion(bf16[192,1024]{1,0:T(8,128)(2,1)S(1)} %attend.1, bf16[1024,4096]{1,0:T(8,128)(2,1)} %param.27), kind=kOutput, calls=%fused_computation.1 | convolution fusion | flops 1611399168 | bytes 10354688 | tf_op jit(solution)/shard_map/dot_general | solution.py:675
  73.0 45.8 %mix_rows.1 = (bf16[48,4096]{1,0:T(8,128)(2,1)}, bf16[4,48,4096]{2,1,0:T(8,128)(2,1)}, f32[4,48,128]{2,1,0:T(8,128)}) custom-call(bf16[4,48,4096]{2,1,0:T(8,128)(2,1)} %bitcast.40, bf16[48,4096]{1,0:T(8,128)(2,1)} %resid.1, f32[1,4096]{1,0:T(1,128)} %bitcast.49, f32[1,4096]{1,0:T(1,128)} %bitcast.50, f32[48,128]{1,0:T(8,128)} %maximum_maximum_fusion.side), custom_call_target="tpu_custom_call" | custom-call | tf_op jit(solution)/shard_map/mix_rows/pallas_call | solution.py:255
  118.8 1.2 fusion.24
  120.1 0.1 copy.55
  120.1 0.1 copy.56
  120.2 0.1 copy.54
  120.3 0.1 copy.57
  120.4 1.4 copy-done.1
  121.8 1.6 copy-done.7
  123.4 1.6 copy-done.8
  125.0 1.5 shared.1
  126.6 1.8 convolution_convert_fusion
  128.4 80.0 %dispatch.1 = bf16[32,24,4096]{2,1,0:T(8,128)(2,1)S(1)} custom-call(bf16[32,24,4096]{2,1,0:T(8,128)(2,1)S(1)} %bitcast.29), custom_call_target="tpu_custom_call" | custom-call | tf_op jit(solution)/shard_map/dispatch/pallas_call | solution.py:373
  208.5 6.2 %expert.1 = bf16[768,4096]{1,0:T(8,128)(2,1)S(1)} custom-call(bf16[768,4096]{1,0:T(8,128)(2,1)S(1)} %bitcast.31, bf16[4096,256]{1,0:T(8,128)(2,1)S(1)} %bitcast.35, bf16[4096,256]{1,0:T(8,128)(2,1)S(1)} %bitcast.36, bf16[256,4096]{1,0:T(8,128)(2,1)S(1)} %bitcast.37), custom_call_target="tpu_custom_call" | custom-call | tf_op jit(solution)/shard_map/expert/pallas_call | solution.py:610
  214.7 59.3 %bring.1 = bf16[32,24,2560]{2,1,0:T(8,128)(2,1)S(1)} custom-call(bf16[32,24,4096]{2,1,0:T(8,128)(2,1)S(1)} %bitcast.32), custom_call_target="tpu_custom_call" | custom-call | tf_op jit(solution)/shard_map/bring/pallas_call | solution.py:452
  274.0 1.0 fusion.19
  275.0 1.0 convolution_add_fusion
  276.1 0.2 slice_select_fusion.3
  276.3 0.5 fusion
  276.8 1.3 pad_maximum_fusion
  278.1 24.0 %finish.1 = bf16[48,4096]{1,0:T(8,128)(2,1)} custom-call(bf16[4,48,4096]{2,1,0:T(8,128)(2,1)} %bitcast.38, bf16[48,4096]{1,0:T(8,128)(2,1)} %get-tuple-element.10.mixed, f32[1,4096]{1,0:T(1,128)} %bitcast.51), custom_call_target="tpu_custom_call" | custom-call | tf_op jit(solution)/shard_map/finish/pallas_call | solution.py:290
  302.2 1.8 copy.59
  (29 shorter events, 0.2 us)
Async XLA Ops:
  0.0 7.6 %copy-start.12 = (bf16[192,512]{1,0:T(8,128)(2,1)S(1)}, bf16[192,512]{1,0:T(8,128)(2,1)}, u32[]{:S(2)}) copy-start(bf16[192,512]{1,0:T(8,128)(2,1)} %param.21) | copy-start | bytes 589828
  8.0 34.5 %copy-start.9 = (bf16[512,1024]{1,0:T(8,128)(2,1)S(1)}, bf16[512,1024]{1,0:T(8,128)(2,1)}, u32[]{:S(2)}) copy-start(bf16[512,1024]{1,0:T(8,128)(2,1)} %wk_ref.1) | copy-start | bytes 3145732
  8.1 34.5 %copy-start.10 = (bf16[512,1024]{1,0:T(8,128)(2,1)S(1)}, bf16[512,1024]{1,0:T(8,128)(2,1)}, u32[]{:S(2)}) copy-start(bf16[512,1024]{1,0:T(8,128)(2,1)} %wv_ref.1) | copy-start | bytes 3145732
  8.1 34.5 %copy-start.11 = (bf16[192,1024]{1,0:T(8,128)(2,1)S(1)}, bf16[192,1024]{1,0:T(8,128)(2,1)}, u32[]{:S(2)}) copy-start(bf16[192,1024]{1,0:T(8,128)(2,1)} %qn_ref.1) | copy-start | bytes 1179652
  39.4 3.1 %copy-start = (bf16[32,192,640]{2,1,0:T(8,128)(2,1)}, bf16[32,192,640]{2,1,0:T(8,128)(2,1)S(1)}, u32[]{:S(2)}) copy-start(bf16[32,192,640]{2,1,0:T(8,128)(2,1)S(1)} %gather_latents.1) | copy-start | bytes 23592964
  73.0 47.4 %copy-start.6 = (bf16[4096,256]{1,0:T(8,128)(2,1)S(1)}, bf16[4096,256]{1,0:T(8,128)(2,1)}, u32[]{:S(2)}) copy-start(bf16[4096,256]{1,0:T(8,128)(2,1)} %gate.1) | copy-start | bytes 6291460
  120.4 1.4 copy-start.1
  121.8 1.6 copy-start.7
  123.4 1.6 copy-start.8
  125.0 1.6 copy-start.2
  128.4 80.0 %copy-start.3 = (bf16[1,4096,256]{2,1,0:T(8,128)(2,1)S(1)}, bf16[1,4096,256]{2,1,0:T(8,128)(2,1)}, u32[]{:S(2)}) copy-start(bf16[1,4096,256]{2,1,0:T(8,128)(2,1)} %param.33) | copy-start | bytes 6291460
  128.4 80.0 %copy-start.4 = (bf16[1,4096,256]{2,1,0:T(8,128)(2,1)S(1)}, bf16[1,4096,256]{2,1,0:T(8,128)(2,1)}, u32[]{:S(2)}) copy-start(bf16[1,4096,256]{2,1,0:T(8,128)(2,1)} %param.34) | copy-start | bytes 6291460
  128.4 80.0 %copy-start.5 = (bf16[1,256,4096]{2,1,0:T(8,128)(2,1)S(1)}, bf16[1,256,4096]{2,1,0:T(8,128)(2,1)}, u32[]{:S(2)}) copy-start(bf16[1,256,4096]{2,1,0:T(8,128)(2,1)} %param.35) | copy-start | bytes 6291460
